TPU v7x, 512 devices: a whole 4x4x16 slice. The times are simulated.
512 devices in a mesh: sp: 64 (over z, y), tp: 8 (over x, core).
Axes of the slice: x: 4, y: 4, z: 16, core: 2. Of those that a mesh axis runs over, the one named last changes fastest.
Arguments:
- tokens: bfloat16 [65536, 2048], P('sp', 'tp'), may hold values from -6 to 6
- norm_gain: float32 [2048], replicated, may hold values from 0.1 to 1.9
- w_conv_a: bfloat16 [2048, 1024], P('sp', 'tp'), may hold values from -0.125 to 0.125
- w_conv_gate: bfloat16 [2048, 1024], P('sp', 'tp'), may hold values from -0.125 to 0.125
- conv_weight: float32 [31, 1024], P(None, 'tp'), may hold values from -16 to 16
- conv_gain: float32 [1024], P('tp'), may hold values from 0.1 to 1.9
- w_query: bfloat16 [2048, 512], P('sp', 'tp'), may hold values from -0.125 to 0.125
- w_key: bfloat16 [2048, 512], P('sp', 'tp'), may hold values from -0.125 to 0.125
- w_value: bfloat16 [2048, 1024], P('sp', 'tp'), may hold values from -0.125 to 0.125
- w_outgate: bfloat16 [2048, 1024], P('sp', 'tp'), may hold values from -0.125 to 0.125
- w_decay: bfloat16 [2048, 512], P('sp', 'tp'), may hold values from -0.125 to 0.125
- decay_bias: float32 [512], P('tp'), may hold values from 0 to 12
- decay_extra: float32 [65536, 512], P('sp', 'tp'), may hold values from -2 to 0
- head_gain: float32 [128], replicated, may hold values from 0.1 to 1.9
- init_state: float32 [8, 64, 128], P('tp'), may hold values from -1536 to 1536
- w_out_conv: bfloat16 [1024, 2048], P('tp', 'sp'), may hold values from -0.125 to 0.125
- w_out_gla: bfloat16 [1024, 2048], P('tp', 'sp'), may hold values from -0.125 to 0.125
Outputs:
- mixed: bfloat16 [65536, 2048], P(('sp', 'tp'))
All inputs are finite; a program needn't handle non-finite values.
Results may differ from a plain program's by a relative error of at most 0.022.
Values may be sent and summed in bfloat16 or wider, within the bound.
A program may use at most 128 MiB of HBM per device.

v0:
```python
import jax
import jax.numpy as jnp
from jax import lax
from jax.sharding import Mesh
from jax.sharding import PartitionSpec as P

D_CONV = 1024
HK = 64
HV = 128
BLOCK = 64
SP = ("sp_0", "sp_1")
SP_TP = ("sp_0", "sp_1", "tp")


epsilon = 1e-06
gate_divisor = 16.0


def passed_along(value, axis, steps):
    count = lax.axis_size(axis)
    first, last = (max(0, -steps), min(count, count - steps))
    return lax.ppermute(value, axis, [(source, source + steps) for source in range(first, last)])


def copy_for_each(array, axis):
    copies = jnp.broadcast_to(array, (lax.axis_size(axis), *array.shape))
    return lax.all_to_all(copies, axis, split_axis=0, concat_axis=0, tiled=True)


def over_copies(array, axis):
    everything = copy_for_each(array, axis)
    return jnp.sum(everything, axis=0)


def packed_total(arrays, axis):
    ends = [0]
    for a in arrays:
        ends.append(ends[-1] + a.size)
    subtotal = over_copies(jnp.concatenate([a.ravel() for a in arrays]), axis)
    return tuple((subtotal[b:e].reshape(a.shape) for a, b, e in zip(arrays, ends, ends[1:])))


def nothing_yet(array, identity):
    return jax.tree.map(
        lambda part, zero: jnp.zeros_like(part) + jnp.asarray(zero, part.dtype), array, identity
    )


def collected_together(array, axis):
    leaves = jax.tree.leaves(array)
    order = sorted(range(len(leaves)), key=lambda k: -leaves[k].size)
    width = (1, *leaves[order[0]].shape)[-1]
    lines = [
        jnp.pad(leaves[k].reshape(-1), (0, -leaves[k].size % width)).reshape(-1, width)
        for k in order
    ]
    both, at, found = (lax.all_gather(jnp.concatenate(lines), axis), 0, {})
    for k, line in zip(order, lines):
        section = both[:, at : at + len(line)].reshape(len(both), -1)
        found[k] = section[:, : leaves[k].size].reshape(-1, *leaves[k].shape)
        at += len(line)
    numbers = iter(range(len(leaves)))
    return jax.tree.map(lambda _: found[next(numbers)], array)


def carried_in(array, axes, combine, identity):
    before = start = nothing_yet(array, identity)
    subtotal = array
    for axis in reversed(axes):
        peers, mine = (lax.axis_size(axis), lax.axis_index(axis))
        pieces = collected_together(
            jax.tree.map(
                lambda part, kind: part.astype(kind), subtotal, (jnp.bfloat16, jnp.bfloat16)
            ),
            axis,
        )
        inside, subtotal = (start, start)
        for k in range(peers):
            passed = k < mine
            subtotal = combine(
                subtotal, jax.tree.map(lambda part, own: part[k].astype(own.dtype), pieces, array)
            )
            inside = jax.tree.map(lambda new, old: jnp.where(passed, new, old), subtotal, inside)
        before = combine(inside, before)
    return before


def sent_together(arrays, axis, dim, along):
    ends, at = ([], 0)
    for a in arrays[:-1]:
        at += a.shape[along]
        ends.append(at)
    both = jnp.concatenate(arrays, axis=along)
    return tuple(jnp.split(lax.all_gather(both, axis, axis=dim, tiled=True), ends, axis=along))


def rows_first(arrays, axis, dims):
    turned = [jnp.moveaxis(a, dim, 0) for a, dim in zip(arrays, dims)]
    both = jnp.concatenate([t.reshape(len(t), -1) for t in turned], axis=1)
    result, at, done = (lax.all_gather(both, axis, axis=0, tiled=True), 0, [])
    for t, dim in zip(turned, dims):
        section = result[:, at : at + t[0].size].reshape(-1, *t.shape[1:])
        done.append(jnp.moveaxis(section, 0, dim))
        at += t[0].size
    return tuple(done)


def project(hidden, weight):
    return jnp.dot(hidden, weight, preferred_element_type=jnp.float32)


def rounded(values_f32):
    return lax.optimization_barrier(values_f32.astype(jnp.bfloat16)).astype(jnp.float32)


def fold_rows(normed, portions):
    return tuple((project(normed, portion) for portion in portions))


def conv_branch(conv_a, conv_gate, conv_weight, conv_gain):
    gated = (rounded(conv_a) * jax.nn.sigmoid(rounded(conv_gate))).astype(jnp.bfloat16)
    rim_rows = conv_weight.shape[0] - 1
    row_count = gated.shape[0]
    earlier = passed_along(gated[row_count - rim_rows :], SP, 1)
    extended = jnp.concatenate([earlier, gated], axis=0).astype(jnp.float32)
    conv_sum = jnp.zeros(gated.shape, jnp.float32)
    for tap_index in range(conv_weight.shape[0]):
        conv_sum = (
            conv_sum + conv_weight[tap_index][None, :] * extended[tap_index : tap_index + row_count]
        )
    row_sums, row_squares = packed_total(
        (jnp.sum(conv_sum, axis=1), jnp.sum(conv_sum * conv_sum, axis=1)), "tp"
    )
    mean_val = (row_sums / D_CONV)[:, None]
    square_mean = (row_squares / D_CONV)[:, None]
    conv_norm = (
        (conv_sum - mean_val) * lax.rsqrt(square_mean - mean_val * mean_val + epsilon) * conv_gain
    )
    return jax.nn.silu(conv_norm).astype(jnp.bfloat16)


def chain_step(earlier, later):
    return (earlier[0] * later[0], earlier[1] * later[0][:, :, None] + later[1])


def gla_branch(
    query, keys, values, out_gate, decay_pre, decay_bias, decay_extra, head_gain, init_state
):
    row_count = query.shape[0]
    local_heads = init_state.shape[0]
    blocks = row_count // BLOCK
    log_decay = jax.nn.log_sigmoid(decay_pre + decay_bias) / gate_divisor + decay_extra

    def to_heads(array, width):
        return array.reshape(blocks, BLOCK, local_heads, width).transpose(0, 2, 1, 3)

    query_heads = to_heads(rounded(query), HK) * HK ** (-0.5)
    key_heads = to_heads(rounded(keys), HK)
    value_heads = to_heads(rounded(values), HV)
    cum_log = jnp.cumsum(to_heads(log_decay, HK), axis=2)
    block_total = cum_log[:, :, -1:, :]
    query_decayed = query_heads * jnp.exp(cum_log)
    key_inverse = key_heads * jnp.exp(-cum_log)
    key_to_end = key_heads * jnp.exp(block_total - cum_log)
    causal = jnp.tril(jnp.ones((BLOCK, BLOCK), dtype=bool))
    scores = jnp.where(causal, jnp.einsum("nhik,nhjk->nhij", query_decayed, key_inverse), 0.0)
    within = jnp.einsum("nhij,nhjv->nhiv", scores, value_heads)

    def advance(state_current, block_items):
        query_block, key_block, value_block, decay_block = block_items
        carried_state = jnp.einsum("yau,yub->yab", query_block, state_current)
        state_following = state_current * decay_block[:, 0, :, None] + jnp.einsum(
            "tie,tis->tes", key_block, value_block
        )
        return (state_following, carried_state)

    zero_state = jnp.zeros(init_state.shape, jnp.float32)
    local_end, carried_out = lax.scan(
        advance, zero_state, (query_decayed, key_to_end, value_heads, jnp.exp(block_total))
    )
    block_sums = block_total[:, :, 0, :]
    device_log = jnp.sum(block_sums, axis=0)
    prefix_log = jnp.cumsum(block_sums, axis=0) - block_sums
    before_decay, before_state = carried_in(
        (jnp.exp(device_log), local_end),
        SP,
        chain_step,
        (jnp.ones_like(device_log), jnp.zeros_like(local_end)),
    )
    state_entering = before_state + init_state * before_decay[:, :, None]
    query_since_beginning = query_decayed * jnp.exp(prefix_log)[:, :, None, :]
    incoming_state = jnp.einsum("oltu,luf->oltf", query_since_beginning, state_entering)
    attn = within + carried_out + incoming_state
    normal_attn = (
        attn * lax.rsqrt(jnp.mean(attn * attn, axis=-1, keepdims=True) + epsilon) * head_gain
    )
    normal_attn = normal_attn.transpose(0, 2, 1, 3).reshape(row_count, local_heads * HV)
    return (normal_attn * jax.nn.silu(rounded(out_gate))).astype(jnp.bfloat16)


def per_device(
    tokens,
    norm_gain,
    w_conv_a,
    w_conv_gate,
    conv_weight,
    conv_gain,
    w_query,
    w_key,
    w_value,
    w_outgate,
    w_decay,
    decay_bias,
    decay_extra,
    head_gain,
    init_state,
    w_out_conv,
    w_out_gla,
):
    features = lax.all_gather(tokens, "tp", axis=1, tiled=True)
    widened = features.astype(jnp.float32)
    normed = (
        widened
        * lax.rsqrt(jnp.mean(widened * widened, axis=-1, keepdims=True) + epsilon)
        * norm_gain
    ).astype(jnp.bfloat16)
    projected = fold_rows(
        normed,
        sent_together(
            (w_conv_a, w_conv_gate, w_query, w_key, w_value, w_outgate, w_decay), SP, 0, 1
        ),
    )
    conv_proj = projected[:2]
    conv_out = conv_branch(conv_proj[0], conv_proj[1], conv_weight, conv_gain)
    gla_proj = projected[2:]
    gla_out = gla_branch(
        gla_proj[0],
        gla_proj[1],
        gla_proj[2],
        gla_proj[3],
        gla_proj[4],
        decay_bias,
        decay_extra,
        head_gain,
        init_state,
    )
    out_conv, out_gla = rows_first((w_out_conv, w_out_gla), SP, (1, 1))
    return lax.psum_scatter(
        (project(conv_out, out_conv) + project(gla_out, out_gla)).astype(jnp.bfloat16),
        "tp",
        scatter_dimension=0,
        tiled=True,
    )


def solution(mesh):
    torus = Mesh(mesh.devices.reshape(16, 4, mesh.shape["tp"]), ("sp_0", "sp_1", "tp"))
    placed = (
        P(SP, "tp"),
        P(),
        P(SP, "tp"),
        P(SP, "tp"),
        P(None, "tp"),
        P("tp"),
        P(SP, "tp"),
        P(SP, "tp"),
        P(SP, "tp"),
        P(SP, "tp"),
        P(SP, "tp"),
        P("tp"),
        P(SP, "tp"),
        P(),
        P("tp", None, None),
        P("tp", SP),
        P("tp", SP),
    )
    return jax.shard_map(
        per_device, mesh=torus, in_specs=placed, out_specs=P(SP_TP, None), check_vma=False
    )
```

profile of v0, /device:TPU:1, one launch (start us, length us, event | category | flops | bytes accessed | tf_op | source)
XLA Modules:
  0.0 399.4 jit_solution(112198304214924607)
XLA Ops:
  12.3 46.1 %all-gather.8.cloned.1.call-done = bf16[1024,2048]{1,0:T(8,128)(2,1)} async-done(((bf16[1024,256]{1,0:T(8,128)(2,1)}), bf16[1024,2048]{1,0:T(8,128)(2,1)}) %all-gather.8.cloned.1.call-update) | async-done | bytes 4194320 | tf_op jit(solution)/shard_map/all_gather | solution.py:220
  58.3 3.2 fusion.11
  61.8 3.0 fusion.13
  64.8 131.6 %all-gather.10.cloned.1.call-done = bf16[2048,704]{1,0:T(8,128)(2,1)} async-done(((bf16[32,704]{1,0:T(8,128)(2,1)}), bf16[2048,704]{1,0:T(8,128)(2,1)}) %all-gather.10.cloned.1.call-update) | async-done | bytes 2883600 | tf_op jit(solution)/shard_map/all_gather | solution.py:94
  196.4 3.7 convolution_convert_fusion.5
  200.4 3.8 convolution_convert_fusion.4
  204.5 4.4 %convolution_convert_fusion.1 = bf16[1024,128]{1,0:T(8,128)(2,1)} fusion(bf16[1024,2048]{1,0:T(8,128)(2,1)} %fusion.13, bf16[2048,704]{1,0:T(8,128)(2,1)} %all-gather.10.cloned.1.call-done), kind=kOutput, calls=%fused_computation.28 | convolution fusion | flops 537001984 | bytes 4980736 | tf_op jit(solution)/shard_map/dot_general | solution.py:109
  208.9 2.5 fusion.68
  212.0 6.3 %fusion.240 = f32[16,1,64,64]{3,0,1,2:T(8,128)S(1)} fusion(f32[16,1,64,64]{3,0,1,2:T(8,128)S(1)} %copy.125), kind=kOutput, calls=%fused_computation.398 | output fusion | flops 4128768 | bytes 524288 | tf_op jit(solution)/shard_map/jit(cumsum)/reduce_window_sum | solution.py:160
  219.9 2.0 fusion.239
  221.9 42.4 %while.13 = (s32[]{:T(128)}, f32[1,64,128]{2,1,0:T(8,128)S(1)}, f32[16,1,64,128]{3,2,1,0:T(8,128)}, f32[16,1,1,64]{3,2,1,0:T(1,128)S(1)}, f32[16,1,64,64]{3,0,1,...) while((s32[]{:T(128)}, f32[1,64,128]{2,1,0:T(8,128)S(1)}, ...), condition=%wide.region_6.7_spmd.clone, body=%wide.region_5.6_spmd.clone.sunk | while | flops 2129923 | bytes 246656 | solution.py:178
  264.4 9.8 %all-gather.2 = bf16[4,65,128]{2,1,0:T(8,128)(2,1)S(1)} all-gather(bf16[1,65,128]{2,1,0:T(8,128)(2,1)S(1)} %maximum_bitcast_fusion), channel_id=2, replica_groups=mesh['sp_0'=16,'sp_1'=4,'tp'=8] {'sp_1'}, dimensions={0}, use_global_device_ids=true | all-gather | bytes 83200 | tf_op jit(solution)/shard_map/all_gather | solution.py:57
  274.9 22.2 %all-gather.3 = bf16[16,65,128]{2,1,0:T(8,128)(2,1)S(1)} all-gather(bf16[1,65,128]{2,1,0:T(8,128)(2,1)S(1)} %maximum_bitcast_fusion.1), channel_id=3, replica_groups=mesh['sp_0'=16,'sp_1'=4,'tp'=8] {'sp_0'}, dimensions={0}, use_global_device_ids=true | all-gather | bytes 282880 | tf_op jit(solution)/shard_map/all_gather | solution.py:57
  299.1 3.7 convolution_convert_fusion.3
  302.9 2.3 convolution_convert_fusion.2
  305.3 2.1 collective-permute-start
  311.7 1.7 multiply_reduce_fusion
  313.3 3.6 convolution_convert_fusion
  317.2 2.4 fusion.237
  320.3 23.6 %all-to-all-start = ((f32[8,1,2048]{2,1,0:T(1,128)}), f32[8,1,2048]{2,1,0:T(1,128)S(1)}, u32[]{:S(2)}, u32[]{:S(2)}) async-start(f32[8,1,2048]{2,1,0:T(1,128)} %broadcast_in_dim.20), calls=%async_computation | async-start | bytes 131072 | tf_op jit(solution)/shard_map/all_to_all | solution.py:27
  344.0 4.7 %all-to-all-done = f32[8,1,2048]{2,1,0:T(1,128)S(1)} async-done(((f32[8,1,2048]{2,1,0:T(1,128)}), f32[8,1,2048]{2,1,0:T(1,128)S(1)}, u32[]{:S(2)}, u32[]{:S(2)}) %all-to-all-start) | async-done | bytes 65568 | tf_op jit(solution)/shard_map/all_to_all | solution.py:27
  348.8 2.4 fusion.27
  351.3 3.2 add_convert_fusion
  354.6 38.3 %reduce-scatter.2.cloned.1.call-done = bf16[128,2048]{1,0:T(8,128)(2,1)} async-done(((bf16[1024,2048]{1,0:T(8,128)(2,1)}), bf16[128,2048]{1,0:T(8,128)(2,1)}) %reduce-scatter.2.cloned.1.call-update) | async-done | bytes 524304 | tf_op jit(solution)/shard_map/reduce_scatter | solution.py:248
  (153 shorter events, 59.2 us)
Async XLA Ops:
  6.5 55.0 %copy-start.6 = (f32[2048]{0:T(1024)S(1)}, f32[2048]{0:T(1024)}, u32[]{:S(2)}) copy-start(f32[2048]{0:T(1024)} %param.20) | copy-start | bytes 24580
  6.5 51.8 %all-gather.8.cloned.1.call-start = ((), (), s32[]{:S(2)}) async-start(), calls=%async_computation.2 | async-start | bytes 4718592 | tf_op jit(solution)/shard_map/all_gather | solution.py:220
  7.3 189.1 %all-gather.10.cloned.1.call-start = ((), (), s32[]{:S(2)}) async-start(), calls=%async_computation.3 | async-start | bytes 3194880 | tf_op jit(solution)/shard_map/all_gather | solution.py:94
  8.8 340.0 %all-gather.12.cloned.1.call-start = ((), (), s32[]{:S(2)}) async-start(), calls=%async_computation.4 | async-start | bytes 1064960 | tf_op jit(solution)/shard_map/all_gather | solution.py:100
  58.3 3.4 copy-start.2
  204.1 4.8 %copy-start.5 = (f32[1024,64]{0,1:T(8,128)S(1)}, f32[1024,64]{0,1:T(8,128)}, u32[]{:S(2)}) copy-start(f32[1024,64]{0,1:T(8,128)} %param.31) | copy-start | bytes 786436
  204.2 4.8 %copy-start.10 = (f32[64]{0:T(128)S(1)}, f32[64]{0:T(128)}, u32[]{:S(2)}) copy-start(f32[64]{0:T(128)} %param.30) | copy-start | bytes 772
  204.5 4.4 %copy-start = (bf16[1024,2048]{1,0:T(8,128)(2,1)S(1)}, bf16[1024,2048]{1,0:T(8,128)(2,1)}, u32[]{:S(2)}) copy-start(bf16[1024,2048]{1,0:T(8,128)(2,1)} %fusion.13) | copy-start | bytes 12582916
  274.7 22.4 %copy-start.8 = (f32[64]{0:T(128)}, f32[64]{0:T(128)S(1)}, u32[]{:S(2)}) copy-start(f32[64]{0:T(128)S(1)} %get-tuple-element.201) | copy-start | bytes 772
  297.1 0.7 copy-start.4
  299.1 3.7 copy-start.1
  305.3 11.8 %collective-permute-start = (bf16[30,128]{1,0:T(8,128)(2,1)S(1)}, bf16[30,128]{1,0:T(8,128)(2,1)S(1)}, u32[]{:S(2)}, u32[]{:S(2)}) collective-permute-start(bf16[30,128]{1,0:T(8,128)(2,1)S(1)} %slice.524), channel_id=1, source_target_pairs={{0,8},{8,16},{16,24},{24,32},{32,40},{40,48},{48,56},{56,64},{64,7... | collective-permute-start | bytes 23048 | tf_op jit(solution)/shard_map/ppermute | solution.py:22
  311.0 5.9 %copy-start.9 = (f32[128]{0:T(128)S(1)}, f32[128]{0:T(128)}, u32[]{:S(2)}) copy-start(f32[128]{0:T(128)} %param.32) | copy-start | bytes 1540
  317.2 31.6 %copy-start.7 = (f32[128]{0:T(128)S(1)}, f32[128]{0:T(128)}, u32[]{:S(2)}) copy-start(f32[128]{0:T(128)} %param.24) | copy-start | bytes 1540
  320.3 28.4 %all-to-all-start = ((f32[8,1,2048]{2,1,0:T(1,128)}), f32[8,1,2048]{2,1,0:T(1,128)S(1)}, u32[]{:S(2)}, u32[]{:S(2)}) async-start(f32[8,1,2048]{2,1,0:T(1,128)} %broadcast_in_dim.20), calls=%async_computation | async-start | bytes 131072 | tf_op jit(solution)/shard_map/all_to_all | solution.py:27
  343.9 49.0 %reduce-scatter.2.cloned.1.call-start = ((), (), s32[]{:S(2)}) async-start(), calls=%async_computation.5 | async-start | bytes 4718592 | tf_op jit(solution)/shard_map/reduce_scatter | solution.py:248
  348.8 2.5 copy-start.3
Sparse Core Ops, SparseCore 0:
  9.4 48.8 all-gather.7
  61.3 135.0 all-gather.9
  199.3 133.9 all-gather.11
  354.7 38.1 reduce-scatter.1
where the time goes:
time: 402 us; the launch traced here: 399 us
  waiting for transfers between devices  221 us (55%)
  matrix products  59.1 us (15%)
  blocking collectives  32 us (8%)
  local copies, waits for them, and re-layouts  25.8 us (6%)
  starting transfers between devices  25.8 us (6%)
  other arithmetic  21.7 us (5%)
  between operations  13.6 us (3%)
    all_gather x1, waiting for transfers between devices, sent_together(): lax.all_gather(both, axis, axis=dim, tiled=True)  132 us
    all_gather x1, waiting for transfers between devices, per_device(): features = lax.all_gather(tokens, 'tp', axis=1, tiled=True)  46.1 us
    reduce_scatter x1, waiting for transfers between devices, per_device(): lax.psum_scatter((project(conv_out, out_conv) + project(gla_out, out_gla)...  38.3 us
    all_gather x2, blocking collectives, collected_together(): both, at, found = (lax.all_gather(jnp.concatenate(lines), axis), 0, {})  32 us
    dot_general x9, matrix products, project(): return jnp.dot(hidden, weight, preferred_element_type=jnp.float32)  29.7 us
    all_to_all x1, starting transfers between devices, copy_for_each(): return lax.all_to_all(copies, axis, split_axis=0, concat_axis=0, tiled=True)  23.6 us
    dynamic_slice x16, local copies, waits for them, and re-layouts, gla_branch(): lax.scan(advance, zero_state, (query_decayed, key_to_end, value_heads, jn...  16.1 us
    dot_general x16, matrix products, advance(): jnp.einsum('tie,tis->tes', key_block, value_block)  14.3 us
  transfers between devices with their start and end apart: 6, of which 4 were waited for; matrix products, arithmetic and copies ran while one was open for 25% of the time, Pallas kernels for 0%

commit v1 on v0

v1 whole, which is shorter than its diff:
```python
import jax
import jax.numpy as jnp
from jax import lax
from jax.experimental import pallas as pl
from jax.experimental.pallas import tpu as pltpu
from jax.sharding import Mesh
from jax.sharding import PartitionSpec as P

D = 2048
D_CONV = 1024
HK = 64
HV = 128
BLOCK = 64
ROWS = 1024
NZ, NY, NX, NC = 16, 4, 4, 2
SP = ("z", "y")
TP = ("x", "c")
SP_TP = ("z", "y", "x", "c")
RA, RM, RT = 96, 176, 240
F32, BF16 = jnp.float32, jnp.bfloat16

epsilon = 1e-06
gate_divisor = 16.0


def remote(src, dst, send, recv, **ids):
    return pltpu.make_async_remote_copy(
        src_ref=src,
        dst_ref=dst,
        send_sem=send,
        recv_sem=recv,
        device_id=ids,
        device_id_type=pl.DeviceIdType.MESH,
    )


class Mover:
    def __init__(self):
        self.sent = []

    def send(self, ref, send, recv, **ids):
        copy = remote(ref, ref, send, recv, **ids)
        copy.start()
        self.sent.append(copy)

    def drain(self):
        for copy in self.sent:
            copy.wait_send()
        self.sent = []


def arrived(ref, send, recv, **ids):
    remote(ref, ref, send, recv, **ids).wait_recv()


def pack_chunk(sp, gain, wa, wg, wq, wk, wv, wo, wd, woc, wog, G):
    row = gain[pl.ds(sp, 1), :]
    r = lax.broadcasted_iota(jnp.int32, (32, 32), 0)
    c = lax.broadcasted_iota(jnp.int32, (32, 32), 1)
    col = jnp.sum(jnp.where(r == c, jnp.broadcast_to(row, (32, 32)), 0.0), axis=1, keepdims=True)

    def scaled(ref):
        return ref[...].astype(F32) * col

    d = scaled(wd)
    G[sp, 0:32] = scaled(wv).astype(BF16)
    G[sp, 32:64] = jnp.concatenate([scaled(wq), scaled(wk)], axis=1).astype(BF16)
    G[sp, 64:96] = scaled(wa).astype(BF16)
    G[sp, 96:112] = jnp.concatenate([d[0:16], d[16:32]], axis=1).astype(BF16)
    G[sp, 112:144] = scaled(wg).astype(BF16)
    G[sp, 144:176] = scaled(wo).astype(BF16)
    G[sp, 176:208] = woc[...].astype(F32).T.astype(BF16)
    G[sp, 208:240] = wog[...].astype(F32).T.astype(BF16)


def gather(z, y, x, c, tokens, G, tok, local, sems):
    (a1s, a1r, a2s, a2r, b1s, b1r, b2s, b2r, xs, xr, ds_, dr) = sems
    sp = z * NY + y
    zr, zl = lax.rem(z + 1, NZ), lax.rem(z + NZ - 1, NZ)
    yr, yl = lax.rem(y + 1, NY), lax.rem(y + NY - 1, NY)
    xr_, xl_ = lax.rem(x + 1, NX), lax.rem(x + NX - 1, NX)
    xo = lax.rem(x + 2, NX)
    co = 1 - c
    m = Mover()

    def slab(xi, ci, half):
        col = pl.multiple_of((xi * NC + ci) * 256, 256)
        return tok.at[pl.ds(half * 512, 512), pl.ds(col, 256)]

    def zc(s):
        return lax.rem(z + s + 2 * NZ, NZ)

    own = pltpu.make_async_copy(
        tokens, tok.at[:, pl.ds(pl.multiple_of((x * NC + c) * 256, 256), 256)], local
    )
    own.start()
    barrier = pltpu.get_barrier_semaphore()
    partners = [dict(x=xr_), dict(x=xl_), dict(c=co), dict(y=yr), dict(y=yl), dict(y=lax.rem(y + 2, NY)), dict(z=zr), dict(z=zl)]
    for ids in partners:
        pl.semaphore_signal(barrier, inc=1, device_id=ids, device_id_type=pl.DeviceIdType.MESH)
    pl.semaphore_wait(barrier, len(partners))

    for d in (1, 3, 2):
        m.send(G.at[sp, 0:RA], a1s.at[d - 1], a1r.at[d - 1], y=lax.rem(y + d, NY))

    def b1(s):
        if 0 <= s < 8:
            m.send(G.at[zc(-s) * NY + y, RA:RT], b1s.at[0, s], b1r.at[0, s], z=zr)
        if 0 <= s < 7:
            m.send(G.at[zc(s) * NY + y, RA:RT], b1s.at[1, s], b1r.at[1, s], z=zl)

    def b1_in(s):
        arrived(G.at[zc(-s) * NY + y, RA:RT], b1s.at[0, 0], b1r.at[0, s - 1], z=zl)
        if s <= 7:
            arrived(G.at[zc(s) * NY + y, RA:RT], b1s.at[0, 0], b1r.at[1, s - 1], z=zr)

    def both(s):
        return [(s, -s)] if s in (0, 8) else [(s, -s), (s + 8, s)]

    def b2(s):
        for k, off in both(s):
            ref = G.at[zc(off) * NY + y, RA:RT]
            m.send(ref, b2s.at[0, k], b2r.at[0, k], y=yr)
            m.send(ref, b2s.at[1, k], b2r.at[1, k], y=yl)

    def b2_forward(s):
        for k, off in both(s):
            first = zc(off) * NY
            arrived(G.at[first + yl, RA:RT], b2s.at[0, 0], b2r.at[0, k], y=yl)
            m.send(G.at[first + yl, RA:RM], b2s.at[2, k], b2r.at[2, k], y=yr)
            arrived(G.at[first + yr, RA:RT], b2s.at[0, 0], b2r.at[1, k], y=yr)
            m.send(G.at[first + yr, RM:RT], b2s.at[3, k], b2r.at[3, k], y=yl)

    def b2_end(s):
        yo = lax.rem(y + 2, NY)
        for k, off in both(s):
            first = zc(off) * NY
            arrived(G.at[first + yo, RA:RM], b2s.at[0, 0], b2r.at[2, k], y=yl)
            arrived(G.at[first + yo, RM:RT], b2s.at[0, 0], b2r.at[3, k], y=yr)

    def a2(s, p):
        if s < 8:
            m.send(G.at[pl.ds(zc(-s) * NY + 2 * p, 2), 0:RA], a2s.at[0, s, p], a2r.at[0, s, p], z=zr)
        if s < 7:
            m.send(G.at[pl.ds(zc(s) * NY + 2 * p, 2), 0:RA], a2s.at[1, s, p], a2r.at[1, s, p], z=zl)

    def a2_in(s, p):
        arrived(G.at[pl.ds(zc(-s) * NY + 2 * p, 2), 0:RA], a2s.at[0, 0, 0], a2r.at[0, s - 1, p], z=zl)
        if s <= 7:
            arrived(G.at[pl.ds(zc(s) * NY + 2 * p, 2), 0:RA], a2s.at[0, 0, 0], a2r.at[1, s - 1, p], z=zr)

    def xsend(ref, k, **ids):
        m.send(ref, xs.at[k], xr.at[k], **ids)

    def xin(ref, k, **ids):
        arrived(ref, xs.at[0], xr.at[k], **ids)

    def pair(ref, k):
        m.send(ref, ds_.at[k], dr.at[k], c=co)

    b1(0)
    own.wait()
    xsend(slab(x, c, 0), 0, x=xr_)
    xsend(slab(x, c, 1), 1, x=xl_)
    xsend(slab(x, c, 1), 2, x=xr_)
    xsend(slab(x, c, 0), 3, x=xl_)
    pair(slab(x, c, 0), 0)
    pair(slab(x, c, 1), 1)
    b2(0)
    for d in (1, 2, 3):
        arrived(G.at[z * NY + lax.rem(y + NY - d, NY), 0:RA], a1s.at[0], a1r.at[d - 1], y=lax.rem(y + NY - d, NY))
    for p in (0, 1):
        a2(0, p)
    for s in range(1, 9):
        b1_in(s)
        b1(s)
        b2(s)
        for p in (0, 1):
            a2_in(s, p)
            a2(s, p)
        b2_forward(s - 1)
        if s == 3:
            xin(slab(xl_, c, 0), 0, x=xl_)
            xsend(slab(xl_, c, 0), 4, x=xr_)
            pair(slab(xl_, c, 0), 2)
            xin(slab(xr_, c, 1), 1, x=xr_)
            xsend(slab(xr_, c, 1), 5, x=xl_)
            pair(slab(xr_, c, 1), 3)
        if s == 6:
            xin(slab(xl_, c, 1), 2, x=xl_)
            pair(slab(xl_, c, 1), 4)
            xin(slab(xr_, c, 0), 3, x=xr_)
            pair(slab(xr_, c, 0), 5)
    b2_forward(8)
    xin(slab(xo, c, 0), 4, x=xl_)
    pair(slab(xo, c, 0), 6)
    xin(slab(xo, c, 1), 5, x=xr_)
    pair(slab(xo, c, 1), 7)
    for s in range(9):
        b2_end(s)
    arrivals = [(x, 0), (x, 1), (xl_, 0), (xr_, 1), (xl_, 1), (xr_, 0), (xo, 0), (xo, 1)]
    for k, (xi, half) in enumerate(arrivals):
        arrived(slab(xi, co, half), ds_.at[0], dr.at[k], c=co)
    m.drain()


GATHER_SEMS = [
    pltpu.SemaphoreType.DMA((3,)),
    pltpu.SemaphoreType.DMA((3,)),
    pltpu.SemaphoreType.DMA((2, 8, 2)),
    pltpu.SemaphoreType.DMA((2, 8, 2)),
    pltpu.SemaphoreType.DMA((2, 8)),
    pltpu.SemaphoreType.DMA((2, 8)),
    pltpu.SemaphoreType.DMA((4, 16)),
    pltpu.SemaphoreType.DMA((4, 16)),
    pltpu.SemaphoreType.DMA((6,)),
    pltpu.SemaphoreType.DMA((6,)),
    pltpu.SemaphoreType.DMA((8,)),
    pltpu.SemaphoreType.DMA((8,)),
]


def spread_weights(G, W):
    def step(k, _):
        rows = pl.ds(pl.multiple_of(k * 256, 256), 256)
        sps = pl.ds(k * 8, 8)
        for at, first in ((0, 64), (128, 112), (256, 0), (384, 144), (512, 32)):
            W[rows, at : at + 128] = G[sps, first : first + 32, :].reshape(256, 128)
        d = G[sps, 96:112, :].astype(F32)
        low = d[:, :, 0:64]
        high = d[:, :, 64:128]
        both = jnp.concatenate([low, high], axis=1).reshape(256, 64)
        both = jnp.concatenate([both, jnp.zeros_like(both)], axis=1)
        W[rows, 640:768] = both.astype(BF16)
        return 0

    lax.fori_loop(0, 8, step, 0)


def first_kernel(tokens, gain, wa, wg, wq, wk, wv, wo, wd, woc, wog, proj, dec, wout, G, tok, W, local, *sems):
    z, y, x, c = (lax.axis_index(n) for n in ("z", "y", "x", "c"))
    pack_chunk(z * NY + y, gain, wa, wg, wq, wk, wv, wo, wd, woc, wog, G)
    gather(z, y, x, c, tokens, G, tok, local, sems)
    spread_weights(G, W)
    wout[...] = G[:, 176:240, :]

    def block(i, _):
        rows = pl.ds(pl.multiple_of(i * 256, 256), 256)
        t = tok[rows, :]
        acc = jnp.zeros((256, 128), F32)
        for k in range(16):
            piece = t[:, k * 128 : k * 128 + 128].astype(F32)
            acc = acc + piece * piece
        scale = lax.rsqrt(jnp.sum(acc, axis=1, keepdims=True) * (1.0 / D) + epsilon)
        for n in range(3):
            part = jnp.dot(t, W[:, n * 256 : n * 256 + 256], preferred_element_type=F32) * scale
            if n < 2:
                proj[rows, n * 256 : n * 256 + 256] = part.astype(BF16)
            else:
                proj[rows, 512:640] = part[:, 0:128].astype(BF16)
                dec[rows, :] = part[:, 128:256]
        return 0

    lax.fori_loop(0, 4, block, 0)


def call_first(tokens, gain, weights):
    vm = pl.BlockSpec(memory_space=pltpu.VMEM)
    return pl.pallas_call(
        first_kernel,
        out_shape=(
            jax.ShapeDtypeStruct((ROWS, 640), BF16),
            jax.ShapeDtypeStruct((ROWS, 128), F32),
            jax.ShapeDtypeStruct((64, 64, 128), BF16),
        ),
        in_specs=[pl.BlockSpec(memory_space=pl.ANY)] + [vm] * 10,
        out_specs=(vm, vm, vm),
        scratch_shapes=[
            pltpu.VMEM((64, RT, 128), BF16),
            pltpu.VMEM((ROWS, D), BF16),
            pltpu.VMEM((D, 768), BF16),
            pltpu.SemaphoreType.DMA,
        ]
        + GATHER_SEMS,
        compiler_params=pltpu.CompilerParams(
            collective_id=0, has_side_effects=True, vmem_limit_bytes=60 * 1024 * 1024
        ),
    )(tokens, gain, *weights)


def passed_along(value, axis, steps):
    count = lax.axis_size(axis)
    first, last = (max(0, -steps), min(count, count - steps))
    return lax.ppermute(value, axis, [(source, source + steps) for source in range(first, last)])


def packed_total(arrays, axis):
    ends = [0]
    for a in arrays:
        ends.append(ends[-1] + a.size)
    array = jnp.concatenate([a.ravel() for a in arrays])
    copies = jnp.broadcast_to(array, (lax.axis_size(axis), *array.shape))
    subtotal = jnp.sum(lax.all_to_all(copies, axis, split_axis=0, concat_axis=0, tiled=True), axis=0)
    return tuple((subtotal[b:e].reshape(a.shape) for a, b, e in zip(arrays, ends, ends[1:])))


def collected_together(array, axis):
    leaves = jax.tree.leaves(array)
    order = sorted(range(len(leaves)), key=lambda k: -leaves[k].size)
    width = (1, *leaves[order[0]].shape)[-1]
    lines = [
        jnp.pad(leaves[k].reshape(-1), (0, -leaves[k].size % width)).reshape(-1, width)
        for k in order
    ]
    both, at, found = (lax.all_gather(jnp.concatenate(lines), axis), 0, {})
    for k, line in zip(order, lines):
        section = both[:, at : at + len(line)].reshape(len(both), -1)
        found[k] = section[:, : leaves[k].size].reshape(-1, *leaves[k].shape)
        at += len(line)
    numbers = iter(range(len(leaves)))
    return jax.tree.map(lambda _: found[next(numbers)], array)


def carried_in(array, axes, combine, identity):
    def fresh():
        return jax.tree.map(
            lambda part, zero: jnp.zeros_like(part) + jnp.asarray(zero, part.dtype), array, identity
        )

    before = start = fresh()
    subtotal = array
    for axis in reversed(axes):
        peers, mine = (lax.axis_size(axis), lax.axis_index(axis))
        pieces = collected_together(
            jax.tree.map(lambda part, kind: part.astype(kind), subtotal, (BF16, BF16)), axis
        )
        inside, subtotal = (start, start)
        for k in range(peers):
            passed = k < mine
            subtotal = combine(
                subtotal, jax.tree.map(lambda part, own: part[k].astype(own.dtype), pieces, array)
            )
            inside = jax.tree.map(lambda new, old: jnp.where(passed, new, old), subtotal, inside)
        before = combine(inside, before)
    return before


def conv_branch(conv_a, conv_gate, conv_weight, conv_gain):
    gated = (conv_a.astype(F32) * jax.nn.sigmoid(conv_gate.astype(F32))).astype(BF16)
    rim_rows = conv_weight.shape[0] - 1
    row_count = gated.shape[0]
    earlier = passed_along(gated[row_count - rim_rows :], SP, 1)
    extended = jnp.concatenate([earlier, gated], axis=0).astype(F32)
    conv_sum = jnp.zeros(gated.shape, F32)
    for tap_index in range(conv_weight.shape[0]):
        conv_sum = (
            conv_sum + conv_weight[tap_index][None, :] * extended[tap_index : tap_index + row_count]
        )
    row_sums, row_squares = packed_total(
        (jnp.sum(conv_sum, axis=1), jnp.sum(conv_sum * conv_sum, axis=1)), TP
    )
    mean_val = (row_sums / D_CONV)[:, None]
    square_mean = (row_squares / D_CONV)[:, None]
    conv_norm = (
        (conv_sum - mean_val) * lax.rsqrt(square_mean - mean_val * mean_val + epsilon) * conv_gain
    )
    return jax.nn.silu(conv_norm).astype(BF16)


def chain_step(earlier, later):
    return (earlier[0] * later[0], earlier[1] * later[0][:, :, None] + later[1])


def gla_branch(query, keys, values, out_gate, decay_pre, decay_bias, decay_extra, head_gain, init_state):
    row_count = query.shape[0]
    local_heads = init_state.shape[0]
    blocks = row_count // BLOCK
    log_decay = jax.nn.log_sigmoid(decay_pre + decay_bias) / gate_divisor + decay_extra

    def to_heads(array, width):
        return array.astype(F32).reshape(blocks, BLOCK, local_heads, width).transpose(0, 2, 1, 3)

    query_heads = to_heads(query, HK) * HK ** (-0.5)
    key_heads = to_heads(keys, HK)
    value_heads = to_heads(values, HV)
    cum_log = jnp.cumsum(to_heads(log_decay, HK), axis=2)
    block_total = cum_log[:, :, -1:, :]
    query_decayed = query_heads * jnp.exp(cum_log)
    key_inverse = key_heads * jnp.exp(-cum_log)
    key_to_end = key_heads * jnp.exp(block_total - cum_log)
    causal = jnp.tril(jnp.ones((BLOCK, BLOCK), dtype=bool))
    scores = jnp.where(causal, jnp.einsum("nhik,nhjk->nhij", query_decayed, key_inverse), 0.0)
    within = jnp.einsum("nhij,nhjv->nhiv", scores, value_heads)

    def advance(state_current, block_items):
        query_block, key_block, value_block, decay_block = block_items
        carried_state = jnp.einsum("yau,yub->yab", query_block, state_current)
        state_following = state_current * decay_block[:, 0, :, None] + jnp.einsum(
            "tie,tis->tes", key_block, value_block
        )
        return (state_following, carried_state)

    zero_state = jnp.zeros(init_state.shape, F32)
    local_end, carried_out = lax.scan(
        advance, zero_state, (query_decayed, key_to_end, value_heads, jnp.exp(block_total))
    )
    block_sums = block_total[:, :, 0, :]
    device_log = jnp.sum(block_sums, axis=0)
    prefix_log = jnp.cumsum(block_sums, axis=0) - block_sums
    before_decay, before_state = carried_in(
        (jnp.exp(device_log), local_end),
        SP,
        chain_step,
        (jnp.ones_like(device_log), jnp.zeros_like(local_end)),
    )
    state_entering = before_state + init_state * before_decay[:, :, None]
    query_since_beginning = query_decayed * jnp.exp(prefix_log)[:, :, None, :]
    incoming_state = jnp.einsum("oltu,luf->oltf", query_since_beginning, state_entering)
    attn = within + carried_out + incoming_state
    normal_attn = (
        attn * lax.rsqrt(jnp.mean(attn * attn, axis=-1, keepdims=True) + epsilon) * head_gain
    )
    normal_attn = normal_attn.transpose(0, 2, 1, 3).reshape(row_count, local_heads * HV)
    return (normal_attn * jax.nn.silu(out_gate.astype(F32))).astype(BF16)


def per_device(
    tokens, norm_gain, w_conv_a, w_conv_gate, conv_weight, conv_gain, w_query, w_key, w_value,
    w_outgate, w_decay, decay_bias, decay_extra, head_gain, init_state, w_out_conv, w_out_gla,
):
    proj, dec, wout = call_first(
        tokens,
        norm_gain.reshape(64, 32),
        (w_conv_a, w_conv_gate, w_query, w_key, w_value, w_outgate, w_decay, w_out_conv, w_out_gla),
    )
    conv_out = conv_branch(proj[:, 0:128], proj[:, 128:256], conv_weight, conv_gain)
    gla_out = gla_branch(
        proj[:, 512:576], proj[:, 576:640], proj[:, 256:384], proj[:, 384:512], dec[:, 0:64],
        decay_bias, decay_extra, head_gain, init_state,
    )
    out_conv = wout[:, 0:32, :].reshape(D, 128)
    out_gla = wout[:, 32:64, :].reshape(D, 128)
    partial = jnp.einsum("rk,nk->rn", conv_out, out_conv, preferred_element_type=F32) + jnp.einsum(
        "rk,nk->rn", gla_out, out_gla, preferred_element_type=F32
    )
    return lax.psum_scatter(partial.astype(BF16), TP, scatter_dimension=0, tiled=True)


def solution(mesh):
    torus = Mesh(mesh.devices.reshape(NZ, NY, NX, NC), ("z", "y", "x", "c"))
    placed = (
        P(SP, TP),
        P(),
        P(SP, TP),
        P(SP, TP),
        P(None, TP),
        P(TP),
        P(SP, TP),
        P(SP, TP),
        P(SP, TP),
        P(SP, TP),
        P(SP, TP),
        P(TP),
        P(SP, TP),
        P(),
        P(TP, None, None),
        P(TP, SP),
        P(TP, SP),
    )
    return jax.shard_map(
        per_device, mesh=torus, in_specs=placed, out_specs=P(SP_TP, None), check_vma=False
    )
```

time: 402 us -> 232 us (0.58)
  waiting for transfers between devices: 221 us -> 46.2 us
  Pallas kernels: 0 us -> 61.6 us
  matrix products: 59.1 us -> 22.7 us
  other arithmetic: 21.7 us -> 10.8 us
  starting transfers between devices: 25.8 us -> 18.9 us
    all_gather x3 -> x0, waiting for transfers between devices: 178 us -> none  [the longest x1 132 us: sent_together(): lax.all_gather(both, axis, axis=dim, tiled=True)]
    pallas_call x0 -> x1, Pallas kernels: none -> 61.6 us  [call_first(): pl.pallas_call(first_kernel, out_shape=(jax.ShapeDtypeStruct((ROWS, 640),...]
    dot_general x9 -> x2, matrix products: 29.7 us -> 4.55 us  [the longest x1 3.23 us: per_device(): jnp.einsum('rk,nk->rn', gla_out, out_gla, preferred_element_type=F32)]
    dot_general x16, matrix products: 14.3 us -> 2.81 us  [advance(): jnp.einsum('tie,tis->tes', key_block, value_block)]
    all_to_all x1, starting transfers between devices: 23.6 us -> 16.5 us  [packed_total(): lax.all_to_all(copies, axis, split_axis=0, concat_axis=0, tiled=True)]
    another operation x1, other arithmetic: 6.33 us -> 1.42 us  [gla_branch(): cum_log = jnp.cumsum(to_heads(log_decay, HK), axis=2)]
  transfers between devices with their start and end apart: 6 -> 3, of which waited for: 4 -> 3; matrix products, arithmetic and copies ran while one was open for 25% -> 0% of each run, Pallas kernels for 0% -> 0%
where the time goes in v1:
time: 232 us; the launch traced here: 230 us
  Pallas kernels  61.6 us (27%)
  waiting for transfers between devices  46.2 us (20%)
  blocking collectives  30.9 us (13%)
  local copies, waits for them, and re-layouts  25.4 us (11%)
  matrix products  22.7 us (10%)
  starting transfers between devices  18.9 us (8%)
  between operations  13.7 us (6%)
  other arithmetic  10.8 us (5%)
    pallas_call x1, Pallas kernels, call_first(): pl.pallas_call(first_kernel, out_shape=(jax.ShapeDtypeStruct((ROWS, 640),...  61.6 us
    reduce_scatter x1, waiting for transfers between devices, per_device(): lax.psum_scatter(partial.astype(BF16), TP, scatter_dimension=0, tiled=True)  40.7 us
    all_gather x2, blocking collectives, collected_together(): both, at, found = (lax.all_gather(jnp.concatenate(lines), axis), 0, {})  30.9 us
    dynamic_slice x16, local copies, waits for them, and re-layouts, gla_branch(): lax.scan(advance, zero_state, (query_decayed, key_to_end, value_heads, jn...  17.3 us
    all_to_all x1, starting transfers between devices, packed_total(): lax.all_to_all(copies, axis, split_axis=0, concat_axis=0, tiled=True)  16.5 us
    dot_general x16, matrix products, advance(): carried_state = jnp.einsum('yau,yub->yab', query_block, state_current)  11.9 us
    all_to_all x1, waiting for transfers between devices, packed_total(): lax.all_to_all(copies, axis, split_axis=0, concat_axis=0, tiled=True)  4.76 us
    unnamed x17, local copies, waits for them, and re-layouts  4.69 us
  transfers between devices with their start and end apart: 3, of which 3 were waited for; matrix products, arithmetic and copies ran while one was open for 0% of the time, Pallas kernels for 0%

profile of v1, /device:TPU:1, one launch (start us, length us, event | category | flops | bytes accessed | tf_op | source)
XLA Modules:
  0.0 230.3 jit_solution(1209125676989405350)
XLA Ops:
  6.6 1.4 reshape.675.gain
  7.9 1.4 copy.130.woc
  9.3 1.4 copy.131.wog
  10.7 1.1 copy.133
  11.9 61.6 %shard_map.163 = (bf16[1024,640]{1,0:T(8,128)(2,1)}, f32[1024,128]{1,0:T(8,128)}, bf16[64,64,128]{2,1,0:T(8,128)(2,1)}) custom-call(bf16[1024,256]{1,0:T(8,128)(2,1)} %tokens.1, f32[64,32]{1,0:T(8,128)} %reshape.675.gain, bf16[32,128]{1,0:T(8,128)(2,1)} %wa.1, bf16[32,128]{1,0:T(8,128)(2,1)} %wg.1, bf16[32,64]{1,0:T(8,128)(2,1)} %wq.1, bf16[32,64]{1,0:T(8,128)(2,1)} %wk.1, ...), custom_call_target="tpu_custom_call" | custom-call | tf_op jit(solution)/shard_map/pallas_call | solution.py:269
  74.6 1.5 fusion.19
  76.1 1.4 fusion.227
  78.7 1.1 copy_multiply_fusion.1
  79.8 32.2 %while.13 = (s32[]{:T(128)}, f32[1,64,128]{2,1,0:T(8,128)S(1)}, f32[16,1,64,128]{3,2,1,0:T(8,128)}, f32[16,1,1,64]{3,2,1,0:T(1,128)S(1)}, f32[16,1,64,64]{3,0,1,...) while((s32[]{:T(128)}, f32[1,64,128]{2,1,0:T(8,128)S(1)}, ...), condition=%wide.region_5.6_spmd.clone, body=%wide.region_4.5_spmd.clone.sunk | while | flops 2129923 | bytes 263296 | solution.py:404
  79.8 1.1 constant_dynamic-slice_fusion.4
  85.8 1.1 constant_dynamic-slice_fusion.4
  91.9 1.1 constant_dynamic-slice_fusion.4
  112.0 9.0 %all-gather.2 = bf16[4,65,128]{2,1,0:T(8,128)(2,1)S(1)} all-gather(bf16[1,65,128]{2,1,0:T(8,128)(2,1)S(1)} %maximum_bitcast_fusion), channel_id=2, replica_groups=mesh['z'=16,'y'=4,'x'=4,'c'=2] {'y'}, dimensions={0}, use_global_device_ids=true | all-gather | bytes 83200 | tf_op jit(solution)/shard_map/all_gather | solution.py:315
  121.2 21.9 %all-gather.3 = bf16[16,65,128]{2,1,0:T(8,128)(2,1)S(1)} all-gather(bf16[1,65,128]{2,1,0:T(8,128)(2,1)S(1)} %maximum_bitcast_fusion.1), channel_id=3, replica_groups=mesh['z'=16,'y'=4,'x'=4,'c'=2] {'z'}, dimensions={0}, use_global_device_ids=true | all-gather | bytes 282880 | tf_op jit(solution)/shard_map/all_gather | solution.py:315
  145.1 1.4 bitcast_multiply_fusion.3
  146.4 1.5 fusion.12
  148.0 1.9 multiply_reduce_fusion
  150.4 2.4 %collective-permute-start = (bf16[30,128]{1,0:T(8,128)(2,1)S(1)}, bf16[30,128]{1,0:T(8,128)(2,1)S(1)}, u32[]{:S(2)}, u32[]{:S(2)}) collective-permute-start(bf16[30,128]{1,0:T(8,128)(2,1)S(1)} %slice.552), channel_id=1, source_target_pairs={{0,8},{8,16},{16,24},{24,32},{32,40},{40,48},{48,56},{56,64},{64,7... | collective-permute-start | bytes 23048 | tf_op jit(solution)/shard_map/ppermute | solution.py:294
  153.6 2.4 %fusion.224 = (f32[1024]{0:T(1024)S(1)}, f32[1024]{0:T(1024)S(1)}, f32[1024,128]{1,0:T(8,128)S(1)}) fusion(f32[1054,128]{1,0:T(8,128)S(1)} %maximum_convert_fusion, f32[128]{0:T(128)S(1)} %get-tuple-element.190, f32[128]{0:T(128)S(1)} %get-tuple-element.191, f32[128]{0:T(128)S(1)} %get-tuple-element.162, f32[128]{0:T(128)S(1)} %get-tuple-element.163, ...), kind=kLoop, calls=%fused_computation.376 | loop fusion | flops 8386560 | bytes 16801280 | tf_op jit(solution)/shard_map/reduce_sum | solution.py:360
  156.7 16.5 %all-to-all-start = ((f32[8,1,2048]{2,1,0:T(1,128)}), f32[8,1,2048]{2,1,0:T(1,128)S(1)}, u32[]{:S(2)}, u32[]{:S(2)}) async-start(f32[8,1,2048]{2,1,0:T(1,128)} %broadcast_in_dim.20), calls=%async_computation | async-start | bytes 131072 | tf_op jit(solution)/shard_map/all_to_all | solution.py:303
  173.4 4.8 %all-to-all-done = f32[8,1,2048]{2,1,0:T(1,128)S(1)} async-done(((f32[8,1,2048]{2,1,0:T(1,128)}), f32[8,1,2048]{2,1,0:T(1,128)S(1)}, u32[]{:S(2)}, u32[]{:S(2)}) %all-to-all-start) | async-done | bytes 65568 | tf_op jit(solution)/shard_map/all_to_all | solution.py:303
  178.2 1.3 fusion.57
  179.5 3.2 %add_convert_fusion = bf16[1024,2048]{1,0:T(8,128)(2,1)} fusion(f32[1024,2048]{1,0:T(8,128)S(1)} %fusion.57, bf16[1024,128]{1,0:T(8,128)(2,1)S(1)} %get-tuple-element.147, bf16[2048,128]{1,0:T(8,128)(2,1)S(1)} %bitcast.233), kind=kOutput, calls=%fused_computation.16 | convolution fusion | flops 541065216 | bytes 13369344 | tf_op jit(solution)/shard_map/rk,nk->rn/dot_general | solution.py:443
  182.8 40.7 %reduce-scatter.2.cloned.1.call-done = bf16[128,2048]{1,0:T(8,128)(2,1)} async-done(((bf16[1024,2048]{1,0:T(8,128)(2,1)}), bf16[128,2048]{1,0:T(8,128)(2,1)}) %reduce-scatter.2.cloned.1.call-update) | async-done | bytes 524304 | tf_op jit(solution)/shard_map/reduce_scatter | solution.py:446
  (113 shorter events, 35.3 us)
Async XLA Ops:
  73.5 4.3 %copy-start = (bf16[1024,640]{1,0:T(8,128)(2,1)S(1)}, bf16[1024,640]{1,0:T(8,128)(2,1)}, u32[]{:S(2)}) copy-start(bf16[1024,640]{1,0:T(8,128)(2,1)} %get-tuple-element.46) | copy-start | bytes 3932164
  79.8 70.1 %copy-start.5 = (f32[128]{0:T(128)S(1)}, f32[128]{0:T(128)}, u32[]{:S(2)}) copy-start(f32[128]{0:T(128)} %param.32) | copy-start | bytes 1540
  143.1 0.7 copy-start.2
  145.0 7.8 %copy-start.3 = (f32[31,128]{1,0:T(8,128)S(1)}, f32[31,128]{1,0:T(8,128)}, u32[]{:S(2)}) copy-start(f32[31,128]{1,0:T(8,128)} %param.23) | copy-start | bytes 47620
  150.4 3.1 %collective-permute-start = (bf16[30,128]{1,0:T(8,128)(2,1)S(1)}, bf16[30,128]{1,0:T(8,128)(2,1)S(1)}, u32[]{:S(2)}, u32[]{:S(2)}) collective-permute-start(bf16[30,128]{1,0:T(8,128)(2,1)S(1)} %slice.552), channel_id=1, source_target_pairs={{0,8},{8,16},{16,24},{24,32},{32,40},{40,48},{48,56},{56,64},{64,7... | collective-permute-start | bytes 23048 | tf_op jit(solution)/shard_map/ppermute | solution.py:294
  153.6 19.6 %copy-start.1 = (bf16[64,64,128]{2,1,0:T(8,128)(2,1)S(1)}, bf16[64,64,128]{2,1,0:T(8,128)(2,1)}, u32[]{:S(2)}) copy-start(bf16[64,64,128]{2,1,0:T(8,128)(2,1)} %get-tuple-element.47) | copy-start | bytes 3145732
  153.6 24.6 %copy-start.4 = (f32[128]{0:T(128)S(1)}, f32[128]{0:T(128)}, u32[]{:S(2)}) copy-start(f32[128]{0:T(128)} %param.24) | copy-start | bytes 1540
  156.7 21.4 %all-to-all-start = ((f32[8,1,2048]{2,1,0:T(1,128)}), f32[8,1,2048]{2,1,0:T(1,128)S(1)}, u32[]{:S(2)}, u32[]{:S(2)}) async-start(f32[8,1,2048]{2,1,0:T(1,128)} %broadcast_in_dim.20), calls=%async_computation | async-start | bytes 131072 | tf_op jit(solution)/shard_map/all_to_all | solution.py:303
  173.3 50.2 %reduce-scatter.2.cloned.1.call-start = ((), (), s32[]{:S(2)}) async-start(), calls=%async_computation.2 | async-start | bytes 4718592 | tf_op jit(solution)/shard_map/reduce_scatter | solution.py:446
Sparse Core Ops, SparseCore 0:
  182.9 40.4 reduce-scatter.1

commit v2 on v1

v2 whole, which is shorter than its diff:
```python
import jax
import jax.numpy as jnp
from jax import lax
from jax.experimental import pallas as pl
from jax.experimental.pallas import tpu as pltpu
from jax.sharding import Mesh
from jax.sharding import PartitionSpec as P

D = 2048
D_CONV = 1024
ROWS = 1024
TAPS = 31
NZ, NY, NX, NC = 16, 4, 4, 2
SP = ("z", "y")
TP = ("x", "c")
SP_TP = ("z", "y", "x", "c")
RA, RM, RT = 96, 176, 240
F32, BF16 = jnp.float32, jnp.bfloat16

epsilon = 1e-06
gate_divisor = 16.0


def remote(src, dst, send, recv, **ids):
    return pltpu.make_async_remote_copy(
        src_ref=src,
        dst_ref=dst,
        send_sem=send,
        recv_sem=recv,
        device_id=ids,
        device_id_type=pl.DeviceIdType.MESH,
    )


class Mover:
    def __init__(self):
        self.sent = []

    def send(self, ref, send, recv, **ids):
        copy = remote(ref, ref, send, recv, **ids)
        copy.start()
        self.sent.append(copy)

    def drain(self):
        for copy in self.sent:
            copy.wait_send()
        self.sent = []


def arrived(ref, send, recv, **ids):
    remote(ref, ref, send, recv, **ids).wait_recv()


def pack_chunk(sp, gain, wa, wg, wq, wk, wv, wo, wd, woc, wog, G):
    row = gain[pl.ds(sp // 4, 1), :]
    r = lax.broadcasted_iota(jnp.int32, (32, 128), 0)
    lane = lax.broadcasted_iota(jnp.int32, (32, 128), 1)
    mine = lane == r + 32 * lax.rem(sp, 4)
    col = jnp.sum(jnp.where(mine, jnp.broadcast_to(row, (32, 128)), 0.0), axis=1, keepdims=True)

    def scaled(ref):
        return ref[...].astype(F32) * col

    d = scaled(wd)
    G[sp, 0:32] = scaled(wv).astype(BF16)
    G[sp, 32:64] = jnp.concatenate([scaled(wq), scaled(wk)], axis=1).astype(BF16)
    G[sp, 64:96] = scaled(wa).astype(BF16)
    G[sp, 96:112] = jnp.concatenate([d[0:16], d[16:32]], axis=1).astype(BF16)
    G[sp, 112:144] = scaled(wg).astype(BF16)
    G[sp, 144:176] = scaled(wo).astype(BF16)
    G[sp, 176:208] = woc[...]
    G[sp, 208:240] = wog[...]


def greet(z, y, x, c):
    barrier = pltpu.get_barrier_semaphore()
    partners = [dict(z=lax.rem(z + d, NZ)) for d in range(1, NZ)]
    partners += [dict(y=lax.rem(y + d, NY)) for d in range(1, NY)]
    partners += [peer(x, c, r) for r in range(1, NX * NC)]
    partners += [following(z, y, 1), following(z, y, -1)]
    for ids in partners:
        pl.semaphore_signal(barrier, inc=1, device_id=ids, device_id_type=pl.DeviceIdType.MESH)
    pl.semaphore_wait(barrier, len(partners))


def peer(x, c, r):
    return dict(x=lax.rem(x + r // 2, NX), c=1 - c if r % 2 else c)


def back_peer(x, c, r):
    return dict(x=lax.rem(x + NX - r // 2, NX), c=1 - c if r % 2 else c)


def following(z, y, d):
    sp = lax.rem(z * NY + y + d + NZ * NY, NZ * NY)
    return dict(z=sp // NY, y=lax.rem(sp, NY))


def gather(z, y, x, c, tokens, G, tok, local, sems, meanwhile):
    (a1s, a1r, a2s, a2r, b1s, b1r, b2s, b2r, xs, xr, ds_, dr) = sems
    sp = z * NY + y
    zr, zl = lax.rem(z + 1, NZ), lax.rem(z + NZ - 1, NZ)
    yr, yl = lax.rem(y + 1, NY), lax.rem(y + NY - 1, NY)
    xr_, xl_ = lax.rem(x + 1, NX), lax.rem(x + NX - 1, NX)
    xo = lax.rem(x + 2, NX)
    co = 1 - c
    m = Mover()

    def slab(xi, ci, half):
        col = pl.multiple_of((xi * NC + ci) * 256, 256)
        return tok.at[pl.ds(half * 512, 512), pl.ds(col, 256)]

    def zc(s):
        return lax.rem(z + s + 2 * NZ, NZ)

    own = pltpu.make_async_copy(
        tokens, tok.at[:, pl.ds(pl.multiple_of((x * NC + c) * 256, 256), 256)], local
    )
    own.start()
    greet(z, y, x, c)

    for d in (1, 3, 2):
        m.send(G.at[sp, 0:RA], a1s.at[d - 1], a1r.at[d - 1], y=lax.rem(y + d, NY))

    def b1(s):
        if 0 <= s < 8:
            m.send(G.at[zc(-s) * NY + y, RA:RT], b1s.at[0, s], b1r.at[0, s], z=zr)
        if 0 <= s < 7:
            m.send(G.at[zc(s) * NY + y, RA:RT], b1s.at[1, s], b1r.at[1, s], z=zl)

    def b1_in(s):
        arrived(G.at[zc(-s) * NY + y, RA:RT], b1s.at[0, 0], b1r.at[0, s - 1], z=zl)
        if s <= 7:
            arrived(G.at[zc(s) * NY + y, RA:RT], b1s.at[0, 0], b1r.at[1, s - 1], z=zr)

    def both(s):
        return [(s, -s)] if s in (0, 8) else [(s, -s), (s + 8, s)]

    def b2(s):
        for k, off in both(s):
            ref = G.at[zc(off) * NY + y, RA:RT]
            m.send(ref, b2s.at[0, k], b2r.at[0, k], y=yr)
            m.send(ref, b2s.at[1, k], b2r.at[1, k], y=yl)

    def b2_forward(s):
        for k, off in both(s):
            first = zc(off) * NY
            arrived(G.at[first + yl, RA:RT], b2s.at[0, 0], b2r.at[0, k], y=yl)
            m.send(G.at[first + yl, RA:RM], b2s.at[2, k], b2r.at[2, k], y=yr)
            arrived(G.at[first + yr, RA:RT], b2s.at[0, 0], b2r.at[1, k], y=yr)
            m.send(G.at[first + yr, RM:RT], b2s.at[3, k], b2r.at[3, k], y=yl)

    def b2_end(s):
        yo = lax.rem(y + 2, NY)
        for k, off in both(s):
            first = zc(off) * NY
            arrived(G.at[first + yo, RA:RM], b2s.at[0, 0], b2r.at[2, k], y=yl)
            arrived(G.at[first + yo, RM:RT], b2s.at[0, 0], b2r.at[3, k], y=yr)

    def a2(s, p):
        if s < 8:
            m.send(G.at[pl.ds(zc(-s) * NY + 2 * p, 2), 0:RA], a2s.at[0, s, p], a2r.at[0, s, p], z=zr)
        if s < 7:
            m.send(G.at[pl.ds(zc(s) * NY + 2 * p, 2), 0:RA], a2s.at[1, s, p], a2r.at[1, s, p], z=zl)

    def a2_in(s, p):
        arrived(G.at[pl.ds(zc(-s) * NY + 2 * p, 2), 0:RA], a2s.at[0, 0, 0], a2r.at[0, s - 1, p], z=zl)
        if s <= 7:
            arrived(G.at[pl.ds(zc(s) * NY + 2 * p, 2), 0:RA], a2s.at[0, 0, 0], a2r.at[1, s - 1, p], z=zr)

    def xsend(ref, k, **ids):
        m.send(ref, xs.at[k], xr.at[k], **ids)

    def xin(ref, k, **ids):
        arrived(ref, xs.at[0], xr.at[k], **ids)

    def pair(ref, k):
        m.send(ref, ds_.at[k], dr.at[k], c=co)

    b1(0)
    own.wait()
    xsend(slab(x, c, 0), 0, x=xr_)
    xsend(slab(x, c, 1), 1, x=xl_)
    xsend(slab(x, c, 1), 2, x=xr_)
    xsend(slab(x, c, 0), 3, x=xl_)
    pair(slab(x, c, 0), 0)
    pair(slab(x, c, 1), 1)
    b2(0)
    for d in (1, 2, 3):
        arrived(G.at[z * NY + lax.rem(y + NY - d, NY), 0:RA], a1s.at[0], a1r.at[d - 1], y=lax.rem(y + NY - d, NY))
    for p in (0, 1):
        a2(0, p)
    meanwhile()
    for s in range(1, 9):
        b1_in(s)
        b1(s)
        b2(s)
        for p in (0, 1):
            a2_in(s, p)
            a2(s, p)
        b2_forward(s - 1)
        if s == 3:
            xin(slab(xl_, c, 0), 0, x=xl_)
            xsend(slab(xl_, c, 0), 4, x=xr_)
            pair(slab(xl_, c, 0), 2)
            xin(slab(xr_, c, 1), 1, x=xr_)
            xsend(slab(xr_, c, 1), 5, x=xl_)
            pair(slab(xr_, c, 1), 3)
        if s == 6:
            xin(slab(xl_, c, 1), 2, x=xl_)
            pair(slab(xl_, c, 1), 4)
            xin(slab(xr_, c, 0), 3, x=xr_)
            pair(slab(xr_, c, 0), 5)
    b2_forward(8)
    xin(slab(xo, c, 0), 4, x=xl_)
    pair(slab(xo, c, 0), 6)
    xin(slab(xo, c, 1), 5, x=xr_)
    pair(slab(xo, c, 1), 7)
    for s in range(9):
        b2_end(s)
    arrivals = [(x, 0), (x, 1), (xl_, 0), (xr_, 1), (xl_, 1), (xr_, 0), (xo, 0), (xo, 1)]
    for k, (xi, half) in enumerate(arrivals):
        arrived(slab(xi, co, half), ds_.at[0], dr.at[k], c=co)
    m.drain()


GATHER_SEMS = [
    pltpu.SemaphoreType.DMA((3,)),
    pltpu.SemaphoreType.DMA((3,)),
    pltpu.SemaphoreType.DMA((2, 8, 2)),
    pltpu.SemaphoreType.DMA((2, 8, 2)),
    pltpu.SemaphoreType.DMA((2, 8)),
    pltpu.SemaphoreType.DMA((2, 8)),
    pltpu.SemaphoreType.DMA((4, 16)),
    pltpu.SemaphoreType.DMA((4, 16)),
    pltpu.SemaphoreType.DMA((6,)),
    pltpu.SemaphoreType.DMA((6,)),
    pltpu.SemaphoreType.DMA((8,)),
    pltpu.SemaphoreType.DMA((8,)),
]


def spread_weights(G, W):
    def step(k, _):
        rows = pl.ds(pl.multiple_of(k * 256, 256), 256)
        sps = pl.ds(k * 8, 8)
        for at, first in ((0, 64), (128, 112), (256, 0), (384, 144), (512, 32)):
            W[rows, at : at + 128] = G[sps, first : first + 32, :].reshape(256, 128)
        d = G[sps, 96:112, :].astype(F32)
        both = jnp.concatenate([d[:, :, 0:64], d[:, :, 64:128]], axis=1).reshape(256, 64)
        W[rows, 640:768] = jnp.concatenate([both, both], axis=1).astype(BF16)
        return 0

    lax.fori_loop(0, 8, step, 0)


def nt(a, b):
    return lax.dot_general(a, b, (((1,), (1,)), ((), ())), preferred_element_type=F32)


def tn(a, b):
    return lax.dot_general(a, b, (((0,), (0,)), ((), ())), preferred_element_type=F32)


def nn(a, b):
    return jnp.dot(a, b, preferred_element_type=F32)


def again(x):
    return x.astype(BF16).astype(F32)


def iota(shape, axis):
    return lax.broadcasted_iota(jnp.int32, shape, axis)


def project_rows(tok, W, gext, v, og, qk, dec):
    def block(i, _):
        first = pl.multiple_of(i * 256, 256)
        rows = pl.ds(first, 256)
        t = tok[rows, :]
        acc = jnp.zeros((256, 128), F32)
        for k in range(16):
            piece = t[:, k * 128 : k * 128 + 128].astype(F32)
            acc = acc + piece * piece
        scale = lax.rsqrt(jnp.sum(acc, axis=1, keepdims=True) * (1.0 / D) + epsilon)
        part = nn(t, W[:, 0:256]) * scale
        gated = again(part[:, 0:128]) * jax.nn.sigmoid(again(part[:, 128:256]))
        gext[pl.ds(first + 32, 256), :] = again(gated)
        part = nn(t, W[:, 256:512]) * scale
        v[rows, :] = part[:, 0:128].astype(BF16)
        og[rows, :] = part[:, 128:256].astype(BF16)
        part = nn(t, W[:, 512:768]) * scale
        qk[rows, :] = again(part[:, 0:128])
        dec[rows, :] = part[:, 128:256]
        return 0

    lax.fori_loop(0, 4, block, 0)


def block_products(i, bias, extra, dec, qk, v, SQ, kv, tots):
    rows = slice(i * 256, i * 256 + 256)
    pre = dec[rows, :] + bias
    log = jnp.minimum(pre, 0.0) - jnp.log1p(jnp.exp(-jnp.abs(pre)))
    cum = log * (1.0 / gate_divisor) + extra[rows, :]
    place = lax.rem(iota((256, 128), 0), 64)
    for s in (1, 2, 4, 8, 16, 32):
        cum = cum + jnp.where(place >= s, pltpu.roll(cum, s, 0), 0.0)
    total = cum.reshape(4, 64, 128)[:, 63:64, :]
    tots[4 * i : 4 * i + 4, :] = total.reshape(4, 128)
    total = jnp.broadcast_to(total, (4, 64, 128)).reshape(256, 128)
    low = iota((256, 128), 1) < 64
    a = qk[rows, :]
    b = pltpu.roll(a, 64, 1)
    q = jnp.where(low, a, b) * 0.125
    k = jnp.where(low, b, a)
    q = q * jnp.exp(cum)
    inverse = k * jnp.exp(-cum)
    to_end = k * jnp.exp(total - cum)
    r, s = iota((256, 256), 0), iota((256, 256), 1)
    same = r // 64 == s // 64
    scores = nt(jnp.where(low, q, 0.0).astype(BF16), inverse.astype(BF16))
    SQ[rows, 0:256] = jnp.where(same & (s <= r), scores, 0.0).astype(BF16)
    SQ[rows, 256:512] = jnp.where(same, jnp.concatenate([q, q], axis=1), 0.0).astype(BF16)
    spread = jnp.where(same, jnp.concatenate([to_end, to_end], axis=1), 0.0).astype(BF16)
    kv[rows, :] = tn(spread, v[rows, :])


def conv_sums(cw, gext, csum, mine):
    for b in range(8):
        acc = jnp.zeros((128, 128), F32)
        for j in range(TAPS):
            acc = acc + cw[j : j + 1, :] * gext[128 * b + 2 + j : 128 * b + 130 + j, :]
        csum[128 * b : 128 * b + 128, :] = acc
        t = acc.T
        mine[b : b + 1, :] = jnp.sum(t, axis=0, keepdims=True)
        mine[8 + b : 9 + b, :] = jnp.sum(t * t, axis=0, keepdims=True)


def conv_finish(cst, square, csum, conv_gain, X):
    both = cst[0]
    for k in range(1, 8):
        both = both + cst[k]
    both = both * (1.0 / D_CONV)
    mean = both[0:8]
    square[0:8, :] = mean
    square[8:16, :] = lax.rsqrt(both[8:16] - mean * mean + epsilon)
    t = square[...].T
    for b in range(8):
        n = (csum[128 * b : 128 * b + 128, :] - t[:, b : b + 1]) * t[:, 8 + b : 9 + b] * conv_gain
        X[128 * b : 128 * b + 128, 0:128] = (n * jax.nn.sigmoid(n)).astype(BF16)


def layer(tokens, gain, wa, wg, cw, conv_gain, wq, wk, wv, wo, wd, bias, extra_t, head_gain, init, woc, wog,
          out, G, tok, W, gext, v, og, qk, dec, extra, SQ, kv, tots, square, csum, cst, hout, hin, ybuf, ztot,
          zbuf, fbuf, Sst, X, pout, pin, s0, s1, s2, r0, r1, fl, fr, facc,
          local, hs, hr, cs, cr, ys, yr, zs, zr, fs, fr_, ps, pr, gs, gr, *sems):
    z, y, x, c = (lax.axis_index(n) for n in ("z", "y", "x", "c"))
    sp = z * NY + y
    tp = x * NC + c
    m = Mover()
    pack_chunk(sp, gain, wa, wg, wq, wk, wv, wo, wd, woc, wog, G)
    zbuf[...] = jnp.zeros_like(zbuf)

    def meanwhile():
        for b in range(8):
            e = extra_t[:, 128 * b : 128 * b + 128]
            extra[128 * b : 128 * b + 128, :] = jnp.concatenate([e, e], axis=0).T
        tots[...] = jnp.zeros_like(tots)
        square[...] = jnp.zeros_like(square)

    gather(z, y, x, c, tokens, G, tok, local, sems, meanwhile)
    spread_weights(G, W)
    project_rows(tok, W, gext, v, og, qk, dec)

    hout[...] = gext[ROWS : ROWS + 32, :].astype(BF16)
    after, ahead = following(z, y, 1), following(z, y, -1)
    halo = remote(hout, hin, hs.at[0], hr.at[0], **after)
    halo.start()

    b2 = jnp.concatenate([bias[...], bias[...]], axis=1)
    for i in range(4):
        block_products(i, b2, extra, dec, qk, v, SQ, kv, tots)
    tt = tots[...].T[0:64, :]
    decay = jnp.exp(tt)
    state = jnp.zeros((64, 128), F32)
    for b in range(16):
        state = state * decay[:, b : b + 1] + kv[64 * b : 64 * b + 64, :]
    ybuf[y, 0:64] = state.astype(BF16)
    ybuf[y, 64:128] = jnp.broadcast_to(jnp.exp(jnp.sum(tt, axis=1, keepdims=True)), (64, 128)).astype(BF16)
    for d in (1, 3, 2):
        m.send(ybuf.at[y], ys.at[d - 1], yr.at[d - 1], y=lax.rem(y + d, NY))

    halo.wait_send()
    remote(hout, hin, hs.at[0], hr.at[0], **ahead).wait_recv()
    gext[0:32, :] = jnp.where(sp > 0, hin[...].astype(F32), 0.0)
    conv_sums(cw, gext, csum, cst.at[tp])
    for r in range(1, 8):
        m.send(cst.at[tp], cs.at[r - 1], cr.at[r - 1], **peer(x, c, r))

    for d in (1, 2, 3):
        yd = lax.rem(y + NY - d, NY)
        arrived(ybuf.at[yd], ys.at[0], yr.at[d - 1], y=yd)
    row_state = jnp.zeros((64, 128), F32)
    row_decay = jnp.ones((64, 128), F32)
    pre_state, pre_decay = row_state, row_decay
    for k in range(NY):
        pre_state = jnp.where(y == k, row_state, pre_state)
        pre_decay = jnp.where(y == k, row_decay, pre_decay)
        a = ybuf[k, 64:128].astype(F32)
        row_state = row_state * a + ybuf[k, 0:64].astype(F32)
        row_decay = row_decay * a
    ztot[0] = row_state
    ztot[1] = row_decay
    ztot[2] = pre_state
    ztot[3] = pre_decay
    part = pl.ds(pl.multiple_of(y * 16, 16), 16)
    zbuf[z, 0:16] = ztot[0, part, :].astype(BF16)
    zbuf[z, 16:32] = ztot[1, part, :].astype(BF16)
    for d in range(1, NZ):
        @pl.when(z + d < NZ)
        def _():
            remote(zbuf.at[z], zbuf.at[z], zs.at[d - 1], zr.at[d - 1], z=lax.rem(z + d, NZ)).start()

    for r in range(1, 8):
        ids = back_peer(x, c, r)
        arrived(cst.at[ids["x"] * NC + ids["c"]], cs.at[0], cr.at[r - 1], **ids)
    conv_finish(cst, square, csum, conv_gain[...], X)

    for d in range(1, NZ):
        @pl.when(z >= d)
        def _():
            zd = lax.rem(z + NZ - d, NZ)
            arrived(zbuf.at[zd], zs.at[0], zr.at[d - 1], z=zd)
    state = init[part, :]
    for k in range(NZ - 1):
        following_state = state * zbuf[k, 16:32].astype(F32) + zbuf[k, 0:16].astype(F32)
        state = jnp.where(k < z, following_state, state)
    fbuf[y] = state.astype(BF16)
    for d in (1, 3, 2):
        m.send(fbuf.at[y], fs.at[d - 1], fr_.at[d - 1], y=lax.rem(y + d, NY))
    for d in (1, 2, 3):
        yd = lax.rem(y + NY - d, NY)
        arrived(fbuf.at[yd], fs.at[0], fr_.at[d - 1], y=yd)
    state = fbuf[...].reshape(64, 128).astype(F32) * ztot[3] + ztot[2]
    for b in range(16):
        Sst[64 * b : 64 * b + 64, :] = state.astype(BF16)
        state = state * decay[:, b : b + 1] + kv[64 * b : 64 * b + 64, :]
    for i in range(4):
        rows = slice(256 * i, 256 * i + 256)
        attn = nn(SQ[rows, 0:256], v[rows, :]) + nn(SQ[rows, 256:512], Sst[rows, :])
        mean = jnp.sum(attn * attn, axis=1, keepdims=True) * (1.0 / 128.0)
        o = og[rows, :].astype(F32)
        X[rows, 128:256] = (
            attn * lax.rsqrt(mean + epsilon) * head_gain[...] * (o * jax.nn.sigmoid(o))
        ).astype(BF16)

    xr, xl, xo = lax.rem(x + 1, NX), lax.rem(x + NX - 1, NX), lax.rem(x + 2, NX)
    order = (xo, xr, xl, x)

    def product(xi, ci, n):
        rows = pl.ds(pl.multiple_of((xi * NC + ci) * 128, 128), 128)
        w = jnp.concatenate(
            [
                G[16 * n : 16 * n + 16, 176:208, :].reshape(512, 128),
                G[16 * n : 16 * n + 16, 208:240, :].reshape(512, 128),
            ],
            axis=1,
        )
        return nt(X[rows, :], w)

    def for_pair(q):
        for n in range(4):
            pout[q, :, 512 * n : 512 * n + 512] = product(order[q], 1 - c, n).astype(BF16)
        copy = remote(pout.at[q], pin.at[q], ps.at[q], pr.at[q], c=1 - c)
        copy.start()
        m.sent.append(copy)

    def pair_sum(q, to):
        remote(pout.at[q], pin.at[q], ps.at[q], pr.at[q], c=1 - c).wait_recv()
        for n in range(4):
            cols = slice(512 * n, 512 * n + 512)
            to[:, cols] = (product(order[q], c, n) + pin[q, :, cols].astype(F32)).astype(to.dtype)

    def ring(k, src, dst, xi):
        copy = remote(src, dst, gs.at[k], gr.at[k], x=xi)
        copy.start()
        m.sent.append(copy)

    def ring_in(k, dst, xi):
        remote(dst, dst, gs.at[k], gr.at[k], x=xi).wait_recv()

    top, low = pl.ds(0, 64), pl.ds(64, 64)
    for_pair(0)
    for_pair(1)
    pair_sum(0, s0)
    ring(0, s0.at[top], r0, xr)
    ring(1, s0.at[low], r1, xl)
    for_pair(2)
    pair_sum(1, s1)
    ring(2, s1.at[low], fl.at[low], xr)
    pair_sum(2, s2)
    ring(3, s2.at[top], fr.at[top], xl)
    for_pair(3)
    pair_sum(3, facc)
    ring_in(0, r0, xl)
    s1[0:64, :] = (s1[0:64, :].astype(F32) + r0[...].astype(F32)).astype(BF16)
    ring(4, s1.at[top], fl.at[top], xr)
    ring_in(1, r1, xr)
    s2[64:128, :] = (s2[64:128, :].astype(F32) + r1[...].astype(F32)).astype(BF16)
    ring(5, s2.at[low], fr.at[low], xl)
    ring_in(2, fl.at[low], xl)
    ring_in(3, fr.at[top], xr)
    ring_in(4, fl.at[top], xl)
    out[0:64, :] = (facc[0:64, :] + fl[0:64, :].astype(F32) + fr[0:64, :].astype(F32)).astype(BF16)
    ring_in(5, fr.at[low], xr)
    out[64:128, :] = (facc[64:128, :] + fl[64:128, :].astype(F32) + fr[64:128, :].astype(F32)).astype(BF16)
    m.drain()
    for d in range(1, NZ):
        @pl.when(z + d < NZ)
        def _():
            remote(zbuf.at[z], zbuf.at[z], zs.at[d - 1], zr.at[d - 1], z=lax.rem(z + d, NZ)).wait_send()


def per_device(
    tokens, norm_gain, w_conv_a, w_conv_gate, conv_weight, conv_gain, w_query, w_key, w_value,
    w_outgate, w_decay, decay_bias, decay_extra, head_gain, init_state, w_out_conv, w_out_gla,
):
    vm = pl.BlockSpec(memory_space=pltpu.VMEM)
    dma = pltpu.SemaphoreType.DMA
    scratch = [
        pltpu.VMEM((64, RT, 128), BF16),
        pltpu.VMEM((ROWS, D), BF16),
        pltpu.VMEM((D, 768), BF16),
        pltpu.VMEM((ROWS + 32, 128), F32),
        pltpu.VMEM((ROWS, 128), BF16),
        pltpu.VMEM((ROWS, 128), BF16),
        pltpu.VMEM((ROWS, 128), F32),
        pltpu.VMEM((ROWS, 128), F32),
        pltpu.VMEM((ROWS, 128), F32),
        pltpu.VMEM((ROWS, 512), BF16),
        pltpu.VMEM((ROWS, 128), F32),
        pltpu.VMEM((128, 128), F32),
        pltpu.VMEM((128, 128), F32),
        pltpu.VMEM((ROWS, 128), F32),
        pltpu.VMEM((8, 16, 128), F32),
        pltpu.VMEM((32, 128), BF16),
        pltpu.VMEM((32, 128), BF16),
        pltpu.VMEM((NY, 128, 128), BF16),
        pltpu.VMEM((4, 64, 128), F32),
        pltpu.VMEM((NZ, 32, 128), BF16),
        pltpu.VMEM((NY, 16, 128), BF16),
        pltpu.VMEM((ROWS, 128), BF16),
        pltpu.VMEM((ROWS, 256), BF16),
        pltpu.VMEM((4, 128, D), BF16),
        pltpu.VMEM((4, 128, D), BF16),
        pltpu.VMEM((128, D), BF16),
        pltpu.VMEM((128, D), BF16),
        pltpu.VMEM((128, D), BF16),
        pltpu.VMEM((64, D), BF16),
        pltpu.VMEM((64, D), BF16),
        pltpu.VMEM((128, D), BF16),
        pltpu.VMEM((128, D), BF16),
        pltpu.VMEM((128, D), F32),
        dma,
    ] + [dma((n,)) for n in (1, 1, 7, 7, 3, 3, 15, 15, 3, 3, 4, 4, 6, 6)]
    return pl.pallas_call(
        layer,
        out_shape=jax.ShapeDtypeStruct((128, D), BF16),
        in_specs=[pl.BlockSpec(memory_space=pl.ANY)] + [vm] * 16,
        out_specs=vm,
        scratch_shapes=scratch + GATHER_SEMS,
        compiler_params=pltpu.CompilerParams(
            collective_id=0, has_side_effects=True, vmem_limit_bytes=60 * 1024 * 1024
        ),
    )(
        tokens, norm_gain.reshape(16, 128), w_conv_a, w_conv_gate, conv_weight, conv_gain.reshape(1, 128),
        w_query, w_key, w_value, w_outgate, w_decay, decay_bias.reshape(1, 64), decay_extra.T,
        head_gain.reshape(1, 128), init_state.reshape(64, 128), w_out_conv.T, w_out_gla.T,
    )


def solution(mesh):
    torus = Mesh(mesh.devices.reshape(NZ, NY, NX, NC), ("z", "y", "x", "c"))
    placed = (
        P(SP, TP),
        P(),
        P(SP, TP),
        P(SP, TP),
        P(None, TP),
        P(TP),
        P(SP, TP),
        P(SP, TP),
        P(SP, TP),
        P(SP, TP),
        P(SP, TP),
        P(TP),
        P(SP, TP),
        P(),
        P(TP, None, None),
        P(TP, SP),
        P(TP, SP),
    )
    return jax.shard_map(
        per_device, mesh=torus, in_specs=placed, out_specs=P(SP_TP, None), check_vma=False
    )
```

time: 232 us -> 104 us (0.45)
  waiting for transfers between devices: 46.2 us -> 0 us
  Pallas kernels: 61.6 us -> 102 us
  blocking collectives: 30.9 us -> 0 us
  local copies, waits for them, and re-layouts: 25.4 us -> 1.88 us
  matrix products: 22.7 us -> 0 us
  starting transfers between devices: 18.9 us -> 0 us
  between operations: 13.7 us -> 0.01 us
  other arithmetic: 10.8 us -> 0 us
    reduce_scatter x1 -> x0, waiting for transfers between devices: 40.7 us -> none  [per_device(): lax.psum_scatter(partial.astype(BF16), TP, scatter_dimension=0, tiled=True)]
    pallas_call x1, Pallas kernels: 61.6 us -> 102 us  [per_device(): pl.pallas_call(layer, out_shape=jax.ShapeDtypeStruct((128, D), BF16), in_...]
    all_gather x2 -> x0, blocking collectives: 30.9 us -> none  [collected_together(): both, at, found = (lax.all_gather(jnp.concatenate(lines), axis), 0, {})]
    dot_general x36 -> x0, matrix products: 22.7 us -> none  [the longest x16 11.9 us: advance(): carried_state = jnp.einsum('yau,yub->yab', query_block, state_current)]
    dynamic_slice x16 -> x0, local copies, waits for them, and re-layouts: 17.3 us -> none  [gla_branch(): lax.scan(advance, zero_state, (query_decayed, key_to_end, value_heads, jn...]
    all_to_all x1 -> x0, starting transfers between devices: 16.5 us -> none  [packed_total(): lax.all_to_all(copies, axis, split_axis=0, concat_axis=0, tiled=True)]
    all_to_all x1 -> x0, waiting for transfers between devices: 4.76 us -> none  [packed_total(): lax.all_to_all(copies, axis, split_axis=0, concat_axis=0, tiled=True)]
    mul x5 -> x0, other arithmetic: 3.61 us -> none  [the longest x1 1.38 us: gla_branch(): query_decayed = query_heads * jnp.exp(cum_log)]
  transfers between devices with their start and end apart: 3 -> 0, of which waited for: 3 -> 0; matrix products, arithmetic and copies ran while one was open for 0% -> 0% of each run, Pallas kernels for 0% -> 0%
where the time goes in v2:
time: 104 us
  Pallas kernels  102 us (98%)
  local copies, waits for them, and re-layouts  1.88 us (2%)
    pallas_call x1, Pallas kernels, per_device(): pl.pallas_call(layer, out_shape=jax.ShapeDtypeStruct((128, D), BF16), in_...  102 us

profile of v2, /device:TPU:1, one launch (start us, length us, event | category | flops | bytes accessed | tf_op | source)
XLA Modules:
  0.0 103.8 jit_solution(1508974335052249752)
XLA Ops:
  0.0 101.9 %shard_map.163 = bf16[128,2048]{1,0:T(8,128)(2,1)} custom-call(bf16[1024,256]{1,0:T(8,128)(2,1)} %tokens.1, f32[16,128]{1,0:T(8,128)} %bitcast.10, bf16[32,128]{1,0:T(8,128)(2,1)} %wa.1, bf16[32,128]{1,0:T(8,128)(2,1)} %wg.1, f32[31,128]{1,0:T(8,128)} %cw.1, f32[1,128]{1,0:T(1,128)} %bitcast.13, bf16[32,64]{1,0:T(8,128)(2,1)} %wq.1, bf16[32,64]{1,0:T(8,128)(2,1)} %wk.1, ...), custom_call_target="tpu_custom_call" | custom-call | tf_op jit(solution)/shard_map/pallas_call | solution.py:567
  102.0 1.9 %copy.19 = bf16[128,2048]{1,0:T(8,128)(2,1)} copy(bf16[128,2048]{1,0:T(8,128)(2,1)} %shard_map.163) | data formatting | bytes 1048576

commit v3 on v2

v3 whole, which is shorter than its diff:
```python
import jax
import jax.numpy as jnp
from jax import lax
from jax.experimental import pallas as pl
from jax.experimental.pallas import tpu as pltpu
from jax.sharding import Mesh
from jax.sharding import PartitionSpec as P

D = 2048
D_CONV = 1024
ROWS = 1024
TAPS = 31
NZ, NY, NX, NC = 16, 4, 4, 2
SP = ("z", "y")
TP = ("x", "c")
SP_TP = ("z", "y", "x", "c")
PARTS = ((0, 80), (80, 176), (176, 240))
PAIRS = ((0,), (1, 2), (3, 4), (5, 6), (7, 8))
F32, BF16 = jnp.float32, jnp.bfloat16

epsilon = 1e-06
gate_divisor = 16.0


def remote(src, dst, send, recv, **ids):
    return pltpu.make_async_remote_copy(
        src_ref=src,
        dst_ref=dst,
        send_sem=send,
        recv_sem=recv,
        device_id=ids,
        device_id_type=pl.DeviceIdType.MESH,
    )


class Mover:
    def __init__(self):
        self.sent = []

    def send(self, ref, send, recv, **ids):
        copy = remote(ref, ref, send, recv, **ids)
        copy.start()
        self.sent.append(copy)

    def drain(self):
        for copy in self.sent:
            copy.wait_send()
        self.sent = []


def arrived(ref, send, recv, **ids):
    remote(ref, ref, send, recv, **ids).wait_recv()


def pack_chunk(sp, gain, wa, wg, wq, wk, wv, wo, wd, woc, wog, G):
    row = gain[pl.ds(sp // 4, 1), :]
    r = lax.broadcasted_iota(jnp.int32, (32, 128), 0)
    lane = lax.broadcasted_iota(jnp.int32, (32, 128), 1)
    mine = lane == r + 32 * lax.rem(sp, 4)
    col = jnp.sum(jnp.where(mine, jnp.broadcast_to(row, (32, 128)), 0.0), axis=1, keepdims=True)

    def scaled(ref):
        return ref[...].astype(F32) * col

    d = scaled(wd)
    G[sp, 0:32] = scaled(wv).astype(BF16)
    G[sp, 32:64] = jnp.concatenate([scaled(wq), scaled(wk)], axis=1).astype(BF16)
    G[sp, 64:80] = jnp.concatenate([d[0:16], d[16:32]], axis=1).astype(BF16)
    G[sp, 80:112] = scaled(wa).astype(BF16)
    G[sp, 112:144] = scaled(wg).astype(BF16)
    G[sp, 144:176] = scaled(wo).astype(BF16)
    G[sp, 176:208] = woc[...]
    G[sp, 208:240] = wog[...]


def greet(z, y, x, c):
    barrier = pltpu.get_barrier_semaphore()
    partners = [dict(z=lax.rem(z + d, NZ)) for d in (1, 2, NZ - 2, NZ - 1)]
    partners += [dict(y=lax.rem(y + d, NY)) for d in range(1, NY)]
    partners += [peer(x, c, r) for r in range(1, NX * NC)]
    partners += [following(z, y, 1), following(z, y, -1)]
    for ids in partners:
        pl.semaphore_signal(barrier, inc=1, device_id=ids, device_id_type=pl.DeviceIdType.MESH)
    pl.semaphore_wait(barrier, len(partners))


def peer(x, c, r):
    return dict(x=lax.rem(x + r // 2, NX), c=1 - c if r % 2 else c)


def back_peer(x, c, r):
    return dict(x=lax.rem(x + NX - r // 2, NX), c=1 - c if r % 2 else c)


def following(z, y, d):
    sp = lax.rem(z * NY + y + d + NZ * NY, NZ * NY)
    return dict(z=sp // NY, y=lax.rem(sp, NY))


class Weights:
    def __init__(self, m, z, y, G, zs, zr, ys, yr):
        self.m, self.z, self.y, self.G = m, z, y, G
        self.zs, self.zr, self.ys, self.yr = zs, zr, ys, yr
        self.up, self.down, self.over = (lax.rem(y + d, NY) for d in (1, 3, 2))

    def chunk(self, o, y, first, last):
        return self.G.at[lax.rem(self.z - o + NZ, NZ) * NY + y, first:last]

    def cuts(self, p, o):
        first, last = PARTS[p]
        return first, first + (48, 32)[o % 2] if p == 0 else (first + last) // 2, last

    def z_out(self, p, o):
        step = (2 if abs(o) > 1 else 1) * (1 if o > 0 else -1)
        self.m.send(
            self.chunk(o - step, self.y, *PARTS[p]), self.zs.at[p, o + 7], self.zr.at[p, o + 7], z=lax.rem(self.z + step + NZ, NZ)
        )

    def y_out(self, p, o):
        for k, to in enumerate((self.up, self.down)):
            self.m.send(self.chunk(o, self.y, *PARTS[p]), self.ys.at[p, o + 7, k], self.yr.at[p, o + 7, k], y=to)

    def begin(self, p):
        for o in (1, -1, 2, -2):
            self.z_out(p, o)
        self.y_out(p, 0)

    def offsets(self, pair):
        return [o for a in pair for o in ((a, -a) if a not in (0, 8) else (a,))]

    def relay(self, p, pair):
        for o in self.offsets(pair):
            arrived(self.chunk(o, self.y, *PARTS[p]), self.zs.at[p, 7], self.zr.at[p, o + 7], z=lax.rem(self.z + 1, NZ))
            further = o + 2 if o > 0 else o - 2
            if -7 <= further <= 8:
                self.z_out(p, further)
            self.y_out(p, o)

    def forward(self, p, pair):
        for o in self.offsets(pair):
            first, middle, last = self.cuts(p, o)
            arrived(self.chunk(o, self.down, first, last), self.ys.at[p, 0, 0], self.yr.at[p, o + 7, 0], y=self.down)
            self.m.send(self.chunk(o, self.down, first, middle), self.ys.at[p, o + 7, 2], self.yr.at[p, o + 7, 2], y=self.up)
            arrived(self.chunk(o, self.up, first, last), self.ys.at[p, 0, 0], self.yr.at[p, o + 7, 1], y=self.up)
            self.m.send(self.chunk(o, self.up, middle, last), self.ys.at[p, o + 7, 3], self.yr.at[p, o + 7, 3], y=self.down)

    def end(self, p):
        for pair in PAIRS:
            for o in self.offsets(pair):
                first, middle, last = self.cuts(p, o)
                arrived(self.chunk(o, self.over, first, middle), self.ys.at[p, 0, 0], self.yr.at[p, o + 7, 2], y=self.down)
                arrived(self.chunk(o, self.over, middle, last), self.ys.at[p, 0, 0], self.yr.at[p, o + 7, 3], y=self.up)


class Tokens:
    def __init__(self, m, x, c, tok, ssq, xs, xr, ds, dr):
        self.m, self.c, self.tok, self.ssq = m, c, tok, ssq
        self.xs, self.xr, self.ds, self.dr = xs, xr, ds, dr
        self.x, self.right, self.left, self.over = (lax.rem(x + d, NX) for d in (0, 1, 3, 2))
        self.order = [
            (self.x, 0), (self.x, 1), (self.left, 0), (self.right, 1),
            (self.left, 1), (self.right, 0), (self.over, 0), (self.over, 1),
        ]

    def slab(self, xi, ci, half):
        col = pl.multiple_of((xi * NC + ci) * 256, 256)
        return self.tok.at[pl.ds(half * 512, 512), pl.ds(col, 256)]

    def send(self, xi, half, k, to):
        self.m.send(self.slab(xi, self.c, half), self.xs.at[k], self.xr.at[k], x=to)

    def begin(self):
        self.send(self.x, 0, 0, self.right)
        self.send(self.x, 1, 1, self.left)
        self.send(self.x, 1, 2, self.right)
        self.send(self.x, 0, 3, self.left)
        self.across(0)
        self.across(1)

    def across(self, k):
        self.m.send(self.slab(self.order[k][0], self.c, self.order[k][1]), self.ds.at[k], self.dr.at[k], c=1 - self.c)

    def take(self, k):
        xi, half = self.order[k]
        arrived(self.slab(xi, self.c, half), self.xs.at[0], self.xr.at[k - 2], x=self.right if k % 2 else self.left)
        if k == 2:
            self.send(xi, half, 4, self.right)
        if k == 3:
            self.send(xi, half, 5, self.left)
        self.across(k)

    def take_across(self, k):
        xi, half = self.order[k]
        arrived(self.slab(xi, 1 - self.c, half), self.ds.at[0], self.dr.at[k], c=1 - self.c)

    def squares(self, k, ci):
        xi, half = self.order[k]
        rows = slice(half * 512, half * 512 + 512)
        t = self.slab(xi, ci, half)[...].astype(F32)
        self.ssq[rows, :] += t[:, 0:128] * t[:, 0:128] + t[:, 128:256] * t[:, 128:256]


def unpack_decay(G, Wd):
    def step(k, _):
        rows = pl.ds(pl.multiple_of(k * 256, 256), 256)
        d = G[pl.ds(k * 8, 8), 64:80, :].astype(F32)
        both = jnp.concatenate([d[:, :, 0:64], d[:, :, 64:128]], axis=1).reshape(256, 64)
        Wd[rows, :] = jnp.concatenate([both, both], axis=1).astype(BF16)
        return 0

    lax.fori_loop(0, 8, step, 0)


def column(G, first):
    return G[:, first : first + 32, :].reshape(D, 128)


def nt(a, b):
    return lax.dot_general(a, b, (((1,), (1,)), ((), ())), preferred_element_type=F32)


def tn(a, b):
    return lax.dot_general(a, b, (((0,), (0,)), ((), ())), preferred_element_type=F32)


def nn(a, b):
    return jnp.dot(a, b, preferred_element_type=F32)


def again(x):
    return x.astype(BF16).astype(F32)


def iota(shape, axis):
    return lax.broadcasted_iota(jnp.int32, shape, axis)


def project_first(i, tok, G, Wd, ssq, v, qk, dec):
    rows = slice(256 * i, 256 * i + 256)
    t = tok[rows, :]
    scale = lax.rsqrt(jnp.sum(ssq[rows, :], axis=1, keepdims=True) * (1.0 / D) + epsilon)
    ssq[rows, :] = jnp.broadcast_to(scale, (256, 128))
    part = nn(t, jnp.concatenate([column(G, 0), column(G, 32)], axis=1)) * scale
    v[rows, :] = part[:, 0:128].astype(BF16)
    qk[rows, :] = again(part[:, 128:256])
    dec[rows, :] = nn(t, Wd[...]) * scale


def project_second(i, tok, G, ssq, gext, og):
    rows = slice(256 * i, 256 * i + 256)
    t = tok[rows, :]
    scale = ssq[rows, :]
    part = nn(t, jnp.concatenate([column(G, 80), column(G, 112)], axis=1))
    gated = again(part[:, 0:128] * scale) * jax.nn.sigmoid(again(part[:, 128:256] * scale))
    gext[256 * i + 32 : 256 * i + 288, :] = again(gated)
    og[rows, :] = (nn(t, column(G, 144)) * scale).astype(BF16)


def split_heads(qk, rows):
    low = iota((256, 128), 1) < 64
    a = qk[rows, :]
    b = pltpu.roll(a, 64, 1)
    return low, jnp.where(low, a, b) * 0.125, jnp.where(low, b, a)


def same_block():
    r, s = iota((256, 256), 0), iota((256, 256), 1)
    return r // 64 == s // 64, s <= r


def block_states(i, bias, extra, dec, qk, v, kv, tots):
    rows = slice(i * 256, i * 256 + 256)
    pre = dec[rows, :] + bias
    log = jnp.minimum(pre, 0.0) - jnp.log1p(jnp.exp(-jnp.abs(pre)))
    cum = log * (1.0 / gate_divisor) + extra[rows, :]
    place = lax.rem(iota((256, 128), 0), 64)
    for s in (1, 2, 4, 8, 16, 32):
        cum = cum + jnp.where(place >= s, pltpu.roll(cum, s, 0), 0.0)
    dec[rows, :] = cum
    total = cum.reshape(4, 64, 128)[:, 63:64, :]
    tots[4 * i : 4 * i + 4, :] = total.reshape(4, 128)
    total = jnp.broadcast_to(total, (4, 64, 128)).reshape(256, 128)
    _, _, k = split_heads(qk, rows)
    to_end = k * jnp.exp(total - cum)
    same, _ = same_block()
    spread = jnp.where(same, jnp.concatenate([to_end, to_end], axis=1), 0.0).astype(BF16)
    kv[rows, :] = tn(spread, v[rows, :])


def block_scores(i, dec, qk, v, Q, within):
    rows = slice(i * 256, i * 256 + 256)
    cum = dec[rows, :]
    low, q, k = split_heads(qk, rows)
    q = q * jnp.exp(cum)
    inverse = k * jnp.exp(-cum)
    same, causal = same_block()
    scores = nt(jnp.where(low, q, 0.0).astype(BF16), inverse.astype(BF16))
    scores = jnp.where(same & causal, scores, 0.0).astype(BF16)
    Q[rows, :] = jnp.where(same, jnp.concatenate([q, q], axis=1), 0.0).astype(BF16)
    within[rows, :] = nn(scores, v[rows, :])


def conv_sums(cw, gext, csum, mine):
    for b in range(8):
        acc = jnp.zeros((128, 128), F32)
        for j in range(TAPS):
            acc = acc + cw[j : j + 1, :] * gext[128 * b + 2 + j : 128 * b + 130 + j, :]
        csum[128 * b : 128 * b + 128, :] = acc
        t = acc.T
        mine[b : b + 1, :] = jnp.sum(t, axis=0, keepdims=True)
        mine[8 + b : 9 + b, :] = jnp.sum(t * t, axis=0, keepdims=True)


def conv_finish(cst, square, csum, conv_gain, X):
    both = cst[0]
    for k in range(1, 8):
        both = both + cst[k]
    both = both * (1.0 / D_CONV)
    mean = both[0:8]
    square[0:8, :] = mean
    square[8:16, :] = lax.rsqrt(both[8:16] - mean * mean + epsilon)
    t = square[...].T
    for b in range(8):
        n = (csum[128 * b : 128 * b + 128, :] - t[:, b : b + 1]) * t[:, 8 + b : 9 + b] * conv_gain
        X[128 * b : 128 * b + 128, 0:128] = (n * jax.nn.sigmoid(n)).astype(BF16)


def layer(tokens, gain, wa, wg, cw, conv_gain, wq, wk, wv, wo, wd, bias, extra_t, head_gain, init, woc, wog,
          out, G, tok, Wd, ssq, gext, v, og, qk, dec, extra, Q, within, kv, tots, square, csum, cst, hout, hin, ybuf,
          ztot, zbuf, fbuf, Sst, X, pout, pin, s0, s1, s2, r0, r1, fl, fr, facc,
          local, hs, hr, cs, cr, ys, yr, zs, zr, fs, fr_, ps, pr, gs, gr, xs, xr_, ds, dr, wzs, wzr, wys, wyr):
    z, y, x, c = (lax.axis_index(n) for n in ("z", "y", "x", "c"))
    sp = z * NY + y
    tp = x * NC + c
    m = Mover()
    t = Tokens(m, x, c, tok, ssq, xs, xr_, ds, dr)
    w = Weights(m, z, y, G, wzs, wzr, wys, wyr)
    own = pltpu.make_async_copy(tokens, tok.at[:, pl.ds(pl.multiple_of(tp * 256, 256), 256)], local)
    own.start()
    pack_chunk(sp, gain, wa, wg, wq, wk, wv, wo, wd, woc, wog, G)
    zbuf[...] = jnp.zeros_like(zbuf)
    greet(z, y, x, c)

    w.begin(0)
    own.wait()
    t.begin()
    w.begin(1)
    for b in range(8):
        e = extra_t[:, 128 * b : 128 * b + 128]
        extra[128 * b : 128 * b + 128, :] = jnp.concatenate([e, e], axis=0).T
    tots[...] = jnp.zeros_like(tots)
    square[...] = jnp.zeros_like(square)
    ssq[...] = jnp.zeros_like(ssq)
    t.squares(0, c)
    t.squares(1, c)
    w.relay(0, PAIRS[1])
    w.forward(0, PAIRS[0])
    w.relay(1, PAIRS[1])
    w.relay(0, PAIRS[2])
    w.forward(0, PAIRS[1])
    t.take(2)
    t.take(3)
    w.relay(1, PAIRS[2])
    w.forward(1, PAIRS[0])
    for k in (0, 1):
        t.take_across(k)
        t.squares(k, 1 - c)
    w.relay(0, PAIRS[3])
    w.forward(0, PAIRS[2])
    w.relay(1, PAIRS[3])
    w.forward(1, PAIRS[1])
    w.relay(0, PAIRS[4])
    w.forward(0, PAIRS[3])
    t.take(4)
    t.take(5)
    w.relay(1, PAIRS[4])
    w.begin(2)
    for k in (2, 3):
        t.squares(k, c)
        t.take_across(k)
        t.squares(k, 1 - c)
    w.forward(0, PAIRS[4])
    w.forward(1, PAIRS[2])
    for k in (4, 5):
        t.squares(k, c)
        t.take_across(k)
        t.squares(k, 1 - c)
    t.take(6)
    t.take(7)
    w.end(0)
    unpack_decay(G, Wd)
    for k in (6, 7):
        t.squares(k, c)
        t.take_across(k)
        t.squares(k, 1 - c)

    for i in range(4):
        project_first(i, tok, G, Wd, ssq, v, qk, dec)
        if i == 0:
            w.relay(2, PAIRS[1])
        if i == 2:
            w.forward(1, PAIRS[3])
    b2 = jnp.concatenate([bias[...], bias[...]], axis=1)
    for i in range(4):
        block_states(i, b2, extra, dec, qk, v, kv, tots)
        if i == 1:
            w.relay(2, PAIRS[2])
    tt = tots[...].T[0:64, :]
    decay = jnp.exp(tt)
    state = jnp.zeros((64, 128), F32)
    for b in range(16):
        state = state * decay[:, b : b + 1] + kv[64 * b : 64 * b + 64, :]
    ybuf[y, 0:64] = state.astype(BF16)
    ybuf[y, 64:128] = jnp.broadcast_to(jnp.exp(jnp.sum(tt, axis=1, keepdims=True)), (64, 128)).astype(BF16)
    for d in (1, 3, 2):
        m.send(ybuf.at[y], ys.at[d - 1], yr.at[d - 1], y=lax.rem(y + d, NY))
    w.forward(1, PAIRS[4])
    w.relay(2, PAIRS[3])
    w.end(1)

    for i in range(4):
        project_second(i, tok, G, ssq, gext, og)
        if i == 2:
            w.relay(2, PAIRS[4])
    hout[...] = gext[ROWS : ROWS + 32, :].astype(BF16)
    after, ahead = following(z, y, 1), following(z, y, -1)
    halo = remote(hout, hin, hs.at[0], hr.at[0], **after)
    halo.start()

    for d in (1, 2, 3):
        yd = lax.rem(y + NY - d, NY)
        arrived(ybuf.at[yd], ys.at[0], yr.at[d - 1], y=yd)
    row_state = jnp.zeros((64, 128), F32)
    row_decay = jnp.ones((64, 128), F32)
    pre_state, pre_decay = row_state, row_decay
    for k in range(NY):
        pre_state = jnp.where(y == k, row_state, pre_state)
        pre_decay = jnp.where(y == k, row_decay, pre_decay)
        a = ybuf[k, 64:128].astype(F32)
        row_state = row_state * a + ybuf[k, 0:64].astype(F32)
        row_decay = row_decay * a
    ztot[0] = row_state
    ztot[1] = row_decay
    ztot[2] = pre_state
    ztot[3] = pre_decay
    part = pl.ds(pl.multiple_of(y * 16, 16), 16)
    zbuf[z, 0:16] = ztot[0, part, :].astype(BF16)
    zbuf[z, 16:32] = ztot[1, part, :].astype(BF16)
    for d in range(NZ - 1, 0, -1):
        @pl.when(z + d < NZ)
        def _():
            remote(zbuf.at[z], zbuf.at[z], zs.at[d - 1], zr.at[d - 1], z=lax.rem(z + d, NZ)).start()

    block_scores(0, dec, qk, v, Q, within)
    w.forward(2, PAIRS[0])
    w.forward(2, PAIRS[1])
    halo.wait_send()
    remote(hout, hin, hs.at[0], hr.at[0], **ahead).wait_recv()
    gext[0:32, :] = jnp.where(sp > 0, hin[...].astype(F32), 0.0)
    conv_sums(cw, gext, csum, cst.at[tp])
    for r in range(1, 8):
        m.send(cst.at[tp], cs.at[r - 1], cr.at[r - 1], **peer(x, c, r))
    w.forward(2, PAIRS[2])
    for i in range(1, 4):
        block_scores(i, dec, qk, v, Q, within)
    w.forward(2, PAIRS[3])

    for r in range(1, 8):
        ids = back_peer(x, c, r)
        arrived(cst.at[ids["x"] * NC + ids["c"]], cs.at[0], cr.at[r - 1], **ids)
    conv_finish(cst, square, csum, conv_gain[...], X)

    for d in range(1, NZ):
        @pl.when(z >= d)
        def _():
            zd = lax.rem(z + NZ - d, NZ)
            arrived(zbuf.at[zd], zs.at[0], zr.at[d - 1], z=zd)
    state = init[part, :]
    for k in range(NZ - 1):
        following_state = state * zbuf[k, 16:32].astype(F32) + zbuf[k, 0:16].astype(F32)
        state = jnp.where(k < z, following_state, state)
    fbuf[y] = state.astype(BF16)
    for d in (1, 3, 2):
        m.send(fbuf.at[y], fs.at[d - 1], fr_.at[d - 1], y=lax.rem(y + d, NY))
    w.forward(2, PAIRS[4])
    for d in (1, 2, 3):
        yd = lax.rem(y + NY - d, NY)
        arrived(fbuf.at[yd], fs.at[0], fr_.at[d - 1], y=yd)
    state = fbuf[...].reshape(64, 128).astype(F32) * ztot[3] + ztot[2]
    for b in range(16):
        Sst[64 * b : 64 * b + 64, :] = state.astype(BF16)
        state = state * decay[:, b : b + 1] + kv[64 * b : 64 * b + 64, :]
    for i in range(4):
        rows = slice(256 * i, 256 * i + 256)
        attn = within[rows, :] + nn(Q[rows, :], Sst[rows, :])
        mean = jnp.sum(attn * attn, axis=1, keepdims=True) * (1.0 / 128.0)
        o = og[rows, :].astype(F32)
        X[rows, 128:256] = (
            attn * lax.rsqrt(mean + epsilon) * head_gain[...] * (o * jax.nn.sigmoid(o))
        ).astype(BF16)
    w.end(2)

    right, left, over = lax.rem(x + 1, NX), lax.rem(x + NX - 1, NX), lax.rem(x + 2, NX)
    order = (over, right, left, x)

    def product(xi, ci, n):
        rows = pl.ds(pl.multiple_of((xi * NC + ci) * 128, 128), 128)
        cols = slice(16 * n, 16 * n + 16)
        wt = jnp.concatenate([G[cols, 176:208, :].reshape(512, 128), G[cols, 208:240, :].reshape(512, 128)], axis=1)
        return nt(X[rows, :], wt)

    def half(h):
        return slice(1024 * h, 1024 * h + 1024)

    def pair(q, h):
        return remote(pout.at[q, :, half(h)], pin.at[q, :, half(h)], ps.at[q, h], pr.at[q, h], c=1 - c)

    def for_pair(q, h):
        for n in (2 * h, 2 * h + 1):
            pout[q, :, 512 * n : 512 * n + 512] = product(order[q], 1 - c, n).astype(BF16)
        copy = pair(q, h)
        copy.start()
        m.sent.append(copy)

    def pair_sum(q, h, to):
        mine = [product(order[q], c, n) for n in (2 * h, 2 * h + 1)]
        pair(q, h).wait_recv()
        for n, value in zip((2 * h, 2 * h + 1), mine):
            cols = slice(512 * n, 512 * n + 512)
            to[:, cols] = (value + pin[q, :, cols].astype(F32)).astype(to.dtype)

    def ring(k, src, dst, xi):
        copy = remote(src, dst, gs.at[k], gr.at[k], x=xi)
        copy.start()
        m.sent.append(copy)

    def ring_in(k, dst, xi):
        remote(dst, dst, gs.at[k], gr.at[k], x=xi).wait_recv()

    for_pair(0, 0)
    for_pair(0, 1)
    for_pair(1, 1)
    pair_sum(0, 0, s0)
    ring(0, s0.at[:, half(0)], r0, right)
    pair_sum(0, 1, s0)
    ring(1, s0.at[:, half(1)], r1, left)
    for_pair(2, 0)
    pair_sum(1, 1, s1)
    ring(2, s1.at[:, half(1)], fl.at[:, half(1)], right)
    for_pair(1, 0)
    pair_sum(2, 0, s2)
    ring(3, s2.at[:, half(0)], fr.at[:, half(0)], left)
    for_pair(2, 1)
    pair_sum(1, 0, s1)
    for_pair(3, 0)
    pair_sum(2, 1, s2)
    for_pair(3, 1)
    pair_sum(3, 0, facc)
    pair_sum(3, 1, facc)
    ring_in(0, r0, left)
    s1[:, half(0)] = (s1[:, half(0)].astype(F32) + r0[...].astype(F32)).astype(BF16)
    ring(4, s1.at[:, half(0)], fl.at[:, half(0)], right)
    ring_in(1, r1, right)
    s2[:, half(1)] = (s2[:, half(1)].astype(F32) + r1[...].astype(F32)).astype(BF16)
    ring(5, s2.at[:, half(1)], fr.at[:, half(1)], left)
    ring_in(2, fl.at[:, half(1)], left)
    ring_in(3, fr.at[:, half(0)], right)
    facc[:, half(0)] += fr[:, half(0)].astype(F32)
    facc[:, half(1)] += fl[:, half(1)].astype(F32)
    ring_in(4, fl.at[:, half(0)], left)
    out[:, half(0)] = (facc[:, half(0)] + fl[:, half(0)].astype(F32)).astype(BF16)
    ring_in(5, fr.at[:, half(1)], right)
    out[:, half(1)] = (facc[:, half(1)] + fr[:, half(1)].astype(F32)).astype(BF16)
    m.drain()
    for d in range(1, NZ):
        @pl.when(z + d < NZ)
        def _():
            remote(zbuf.at[z], zbuf.at[z], zs.at[d - 1], zr.at[d - 1], z=lax.rem(z + d, NZ)).wait_send()


def per_device(
    tokens, norm_gain, w_conv_a, w_conv_gate, conv_weight, conv_gain, w_query, w_key, w_value,
    w_outgate, w_decay, decay_bias, decay_extra, head_gain, init_state, w_out_conv, w_out_gla,
):
    vm = pl.BlockSpec(memory_space=pltpu.VMEM)
    dma = pltpu.SemaphoreType.DMA
    shapes = [
        ((64, 240, 128), BF16), ((ROWS, D), BF16), ((D, 128), BF16), ((ROWS, 128), F32), ((ROWS + 32, 128), F32),
        ((ROWS, 128), BF16), ((ROWS, 128), BF16), ((ROWS, 128), F32), ((ROWS, 128), F32), ((ROWS, 128), F32),
        ((ROWS, 256), BF16), ((ROWS, 128), F32), ((ROWS, 128), F32), ((128, 128), F32), ((128, 128), F32),
        ((ROWS, 128), F32), ((8, 16, 128), F32), ((32, 128), BF16), ((32, 128), BF16), ((NY, 128, 128), BF16),
        ((4, 64, 128), F32), ((NZ, 32, 128), BF16), ((NY, 16, 128), BF16), ((ROWS, 128), BF16), ((ROWS, 256), BF16),
        ((4, 128, D), BF16), ((4, 128, D), BF16), ((128, D), BF16), ((128, D), BF16), ((128, D), BF16),
        ((128, 1024), BF16), ((128, 1024), BF16), ((128, D), BF16), ((128, D), BF16), ((128, D), F32),
    ]
    counts = [(1,), (7,), (3,), (15,), (3,), (4, 2), (6,), (6,), (8,), (3, 16), (3, 16, 4)]
    scratch = [pltpu.VMEM(s, t) for s, t in shapes] + [dma] + [dma(n) for n in counts for _ in (0, 1)]
    return pl.pallas_call(
        layer,
        out_shape=jax.ShapeDtypeStruct((128, D), BF16),
        in_specs=[pl.BlockSpec(memory_space=pl.ANY)] + [vm] * 16,
        out_specs=vm,
        scratch_shapes=scratch,
        compiler_params=pltpu.CompilerParams(
            collective_id=0, has_side_effects=True, vmem_limit_bytes=60 * 1024 * 1024
        ),
    )(
        tokens, norm_gain.reshape(16, 128), w_conv_a, w_conv_gate, conv_weight, conv_gain.reshape(1, 128),
        w_query, w_key, w_value, w_outgate, w_decay, decay_bias.reshape(1, 64), decay_extra.T,
        head_gain.reshape(1, 128), init_state.reshape(64, 128), w_out_conv.T, w_out_gla.T,
    )


def solution(mesh):
    torus = Mesh(mesh.devices.reshape(NZ, NY, NX, NC), ("z", "y", "x", "c"))
    placed = (
        P(SP, TP),
        P(),
        P(SP, TP),
        P(SP, TP),
        P(None, TP),
        P(TP),
        P(SP, TP),
        P(SP, TP),
        P(SP, TP),
        P(SP, TP),
        P(SP, TP),
        P(TP),
        P(SP, TP),
        P(),
        P(TP, None, None),
        P(TP, SP),
        P(TP, SP),
    )
    return jax.shard_map(
        per_device, mesh=torus, in_specs=placed, out_specs=P(SP_TP, None), check_vma=False
    )
```

time: 104 us -> 98.6 us (0.948)
  Pallas kernels: 102 us -> 96.5 us
    pallas_call x1, Pallas kernels: 102 us -> 96.5 us  [per_device(): pl.pallas_call(layer, out_shape=jax.ShapeDtypeStruct((128, D), BF16), in_...]
where the time goes in v3:
time: 98.6 us; the launch traced here: 98.4 us
  Pallas kernels  96.5 us (98%)
  local copies, waits for them, and re-layouts  1.88 us (2%)
    pallas_call x1, Pallas kernels, per_device(): pl.pallas_call(layer, out_shape=jax.ShapeDtypeStruct((128, D), BF16), in_...  96.5 us

profile of v3, /device:TPU:1, one launch (start us, length us, event | category | flops | bytes accessed | tf_op | source)
XLA Modules:
  0.0 98.4 jit_solution(13654870041190779611)
XLA Ops:
  0.0 96.5 %shard_map.163 = bf16[128,2048]{1,0:T(8,128)(2,1)} custom-call(bf16[1024,256]{1,0:T(8,128)(2,1)} %tokens.1, f32[16,128]{1,0:T(8,128)} %bitcast.10, bf16[32,128]{1,0:T(8,128)(2,1)} %wa.1, bf16[32,128]{1,0:T(8,128)(2,1)} %wg.1, f32[31,128]{1,0:T(8,128)} %cw.1, f32[1,128]{1,0:T(1,128)} %bitcast.13, bf16[32,64]{1,0:T(8,128)(2,1)} %wq.1, bf16[32,64]{1,0:T(8,128)(2,1)} %wk.1, ...), custom_call_target="tpu_custom_call" | custom-call | tf_op jit(solution)/shard_map/pallas_call | solution.py:598
  96.5 1.9 %copy.19 = bf16[128,2048]{1,0:T(8,128)(2,1)} copy(bf16[128,2048]{1,0:T(8,128)(2,1)} %shard_map.163) | data formatting | bytes 1048576

commit v4 on v3

--- a/solution.py
+++ b/solution.py
@@ -14,7 +14,7 @@
 SP = ("z", "y")
 TP = ("x", "c")
 SP_TP = ("z", "y", "x", "c")
-PARTS = ((0, 80), (80, 176), (176, 240))
+PARTS = ((0, 80), (80, 144), (144, 176), (176, 240))
 PAIRS = ((0,), (1, 2), (3, 4), (5, 6), (7, 8))
 F32, BF16 = jnp.float32, jnp.bfloat16
 
@@ -33,23 +33,16 @@
     )
 
 
-class Mover:
-    def __init__(self):
-        self.sent = []
-
-    def send(self, ref, send, recv, **ids):
-        copy = remote(ref, ref, send, recv, **ids)
-        copy.start()
-        self.sent.append(copy)
-
-    def drain(self):
-        for copy in self.sent:
-            copy.wait_send()
-        self.sent = []
-
-
-def arrived(ref, send, recv, **ids):
-    remote(ref, ref, send, recv, **ids).wait_recv()
+def send(ref, sent, recv, **ids):
+    remote(ref, ref, sent, recv, **ids).start()
+
+
+def arrived(ref, recv, **ids):
+    remote(ref, ref, recv, recv, **ids).wait_recv()
+
+
+def left(ref, sent, **ids):
+    remote(ref, ref, sent, sent, **ids).wait_send()
 
 
 def pack_chunk(sp, gain, wa, wg, wq, wk, wv, wo, wd, woc, wog, G):
@@ -76,9 +69,9 @@
 def greet(z, y, x, c):
     barrier = pltpu.get_barrier_semaphore()
     partners = [dict(z=lax.rem(z + d, NZ)) for d in (1, 2, NZ - 2, NZ - 1)]
-    partners += [dict(y=lax.rem(y + d, NY)) for d in range(1, NY)]
-    partners += [peer(x, c, r) for r in range(1, NX * NC)]
-    partners += [following(z, y, 1), following(z, y, -1)]
+    partners += [dict(y=lax.rem(y + d, NY)) for d in (1, NY - 1)]
+    partners += [dict(x=lax.rem(x + d, NX)) for d in (1, NX - 1)]
+    partners += [dict(c=1 - c)]
     for ids in partners:
         pl.semaphore_signal(barrier, inc=1, device_id=ids, device_id_type=pl.DeviceIdType.MESH)
     pl.semaphore_wait(barrier, len(partners))
@@ -88,73 +81,85 @@
     return dict(x=lax.rem(x + r // 2, NX), c=1 - c if r % 2 else c)
 
 
-def back_peer(x, c, r):
-    return dict(x=lax.rem(x + NX - r // 2, NX), c=1 - c if r % 2 else c)
-
-
 def following(z, y, d):
     sp = lax.rem(z * NY + y + d + NZ * NY, NZ * NY)
     return dict(z=sp // NY, y=lax.rem(sp, NY))
 
 
 class Weights:
-    def __init__(self, m, z, y, G, zs, zr, ys, yr):
-        self.m, self.z, self.y, self.G = m, z, y, G
-        self.zs, self.zr, self.ys, self.yr = zs, zr, ys, yr
+    def __init__(self, z, y, G, zs, zr, ys, yr, fs, fr):
+        self.z, self.y, self.G = z, y, G
+        self.zs, self.zr, self.ys, self.yr, self.fs, self.fr = zs, zr, ys, yr, fs, fr
         self.up, self.down, self.over = (lax.rem(y + d, NY) for d in (1, 3, 2))
 
     def chunk(self, o, y, first, last):
         return self.G.at[lax.rem(self.z - o + NZ, NZ) * NY + y, first:last]
+
+    def several(self, p, n):
+        return self.G.at[0:n, PARTS[p][0] : PARTS[p][1]]
 
     def cuts(self, p, o):
         first, last = PARTS[p]
         return first, first + (48, 32)[o % 2] if p == 0 else (first + last) // 2, last
 
+    def signs(self, a):
+        return (a,) if a in (0, 8) else (a, -a)
+
     def z_out(self, p, o):
         step = (2 if abs(o) > 1 else 1) * (1 if o > 0 else -1)
-        self.m.send(
-            self.chunk(o - step, self.y, *PARTS[p]), self.zs.at[p, o + 7], self.zr.at[p, o + 7], z=lax.rem(self.z + step + NZ, NZ)
-        )
+        send(self.chunk(o - step, self.y, *PARTS[p]), self.zs.at[p], self.zr.at[p, o + 7], z=lax.rem(self.z + step + NZ, NZ))
 
     def y_out(self, p, o):
         for k, to in enumerate((self.up, self.down)):
-            self.m.send(self.chunk(o, self.y, *PARTS[p]), self.ys.at[p, o + 7, k], self.yr.at[p, o + 7, k], y=to)
-
-    def begin(self, p):
+            send(self.chunk(o, self.y, *PARTS[p]), self.ys.at[p], self.yr.at[p, abs(o), k], y=to)
+
+    def begin_z(self, p):
         for o in (1, -1, 2, -2):
             self.z_out(p, o)
+
+    def begin(self, p):
+        self.begin_z(p)
         self.y_out(p, 0)
 
-    def offsets(self, pair):
-        return [o for a in pair for o in ((a, -a) if a not in (0, 8) else (a,))]
-
-    def relay(self, p, pair):
-        for o in self.offsets(pair):
-            arrived(self.chunk(o, self.y, *PARTS[p]), self.zs.at[p, 7], self.zr.at[p, o + 7], z=lax.rem(self.z + 1, NZ))
-            further = o + 2 if o > 0 else o - 2
-            if -7 <= further <= 8:
-                self.z_out(p, further)
-            self.y_out(p, o)
+    def cross(self, p, pair):
+        for a in pair:
+            for o in self.signs(a):
+                self.y_out(p, o)
+
+    def relay(self, p, pair, cross=True):
+        for a in pair:
+            for o in self.signs(a):
+                arrived(self.chunk(o, self.y, *PARTS[p]), self.zr.at[p, o + 7], z=lax.rem(self.z + 1, NZ))
+                further = o + 2 if o > 0 else o - 2
+                if -7 <= further <= 8:
+                    self.z_out(p, further)
+                if cross:
+                    self.y_out(p, o)
 
     def forward(self, p, pair):
-        for o in self.offsets(pair):
-            first, middle, last = self.cuts(p, o)
-            arrived(self.chunk(o, self.down, first, last), self.ys.at[p, 0, 0], self.yr.at[p, o + 7, 0], y=self.down)
-            self.m.send(self.chunk(o, self.down, first, middle), self.ys.at[p, o + 7, 2], self.yr.at[p, o + 7, 2], y=self.up)
-            arrived(self.chunk(o, self.up, first, last), self.ys.at[p, 0, 0], self.yr.at[p, o + 7, 1], y=self.up)
-            self.m.send(self.chunk(o, self.up, middle, last), self.ys.at[p, o + 7, 3], self.yr.at[p, o + 7, 3], y=self.down)
+        for a in pair:
+            both = self.several(p, len(self.signs(a)))
+            arrived(both, self.yr.at[p, a, 0], y=self.down)
+            for o in self.signs(a):
+                first, middle, last = self.cuts(p, o)
+                send(self.chunk(o, self.down, first, middle), self.fs.at[p], self.fr.at[p], y=self.up)
+            arrived(both, self.yr.at[p, a, 1], y=self.up)
+            for o in self.signs(a):
+                first, middle, last = self.cuts(p, o)
+                send(self.chunk(o, self.up, middle, last), self.fs.at[p], self.fr.at[p], y=self.down)
 
     def end(self, p):
-        for pair in PAIRS:
-            for o in self.offsets(pair):
-                first, middle, last = self.cuts(p, o)
-                arrived(self.chunk(o, self.over, first, middle), self.ys.at[p, 0, 0], self.yr.at[p, o + 7, 2], y=self.down)
-                arrived(self.chunk(o, self.over, middle, last), self.ys.at[p, 0, 0], self.yr.at[p, o + 7, 3], y=self.up)
+        arrived(self.several(p, 16), self.fr.at[p], y=self.down)
+
+    def drain(self, p):
+        left(self.several(p, 15), self.zs.at[p], y=self.down)
+        left(self.several(p, 32), self.ys.at[p], y=self.down)
+        left(self.several(p, 16), self.fs.at[p], y=self.down)
 
 
 class Tokens:
-    def __init__(self, m, x, c, tok, ssq, xs, xr, ds, dr):
-        self.m, self.c, self.tok, self.ssq = m, c, tok, ssq
+    def __init__(self, x, c, tok, ssq, xs, xr, ds, dr):
+        self.c, self.tok, self.ssq = c, tok, ssq
         self.xs, self.xr, self.ds, self.dr = xs, xr, ds, dr
         self.x, self.right, self.left, self.over = (lax.rem(x + d, NX) for d in (0, 1, 3, 2))
         self.order = [
@@ -167,7 +172,7 @@
         return self.tok.at[pl.ds(half * 512, 512), pl.ds(col, 256)]
 
     def send(self, xi, half, k, to):
-        self.m.send(self.slab(xi, self.c, half), self.xs.at[k], self.xr.at[k], x=to)
+        send(self.slab(xi, self.c, half), self.xs.at[0], self.xr.at[k], x=to)
 
     def begin(self):
         self.send(self.x, 0, 0, self.right)
@@ -178,11 +183,15 @@
         self.across(1)
 
     def across(self, k):
-        self.m.send(self.slab(self.order[k][0], self.c, self.order[k][1]), self.ds.at[k], self.dr.at[k], c=1 - self.c)
+        send(self.slab(self.order[k][0], self.c, self.order[k][1]), self.ds.at[0], self.dr.at[k], c=1 - self.c)
+
+    def drain(self):
+        left(self.tok.at[:, 0:768], self.xs.at[0], c=1 - self.c)
+        left(self.tok.at[:, 0:1024], self.ds.at[0], c=1 - self.c)
 
     def take(self, k):
         xi, half = self.order[k]
-        arrived(self.slab(xi, self.c, half), self.xs.at[0], self.xr.at[k - 2], x=self.right if k % 2 else self.left)
+        arrived(self.slab(xi, self.c, half), self.xr.at[k - 2], x=self.right if k % 2 else self.left)
         if k == 2:
             self.send(xi, half, 4, self.right)
         if k == 3:
@@ -191,7 +200,7 @@
 
     def take_across(self, k):
         xi, half = self.order[k]
-        arrived(self.slab(xi, 1 - self.c, half), self.ds.at[0], self.dr.at[k], c=1 - self.c)
+        arrived(self.slab(xi, 1 - self.c, half), self.dr.at[k], c=1 - self.c)
 
     def squares(self, k, ci):
         xi, half = self.order[k]
@@ -246,14 +255,18 @@
     dec[rows, :] = nn(t, Wd[...]) * scale
 
 
-def project_second(i, tok, G, ssq, gext, og):
+def project_second(i, tok, G, ssq, gext):
     rows = slice(256 * i, 256 * i + 256)
     t = tok[rows, :]
     scale = ssq[rows, :]
     part = nn(t, jnp.concatenate([column(G, 80), column(G, 112)], axis=1))
     gated = again(part[:, 0:128] * scale) * jax.nn.sigmoid(again(part[:, 128:256] * scale))
     gext[256 * i + 32 : 256 * i + 288, :] = again(gated)
-    og[rows, :] = (nn(t, column(G, 144)) * scale).astype(BF16)
+
+
+def project_third(i, tok, G, ssq, og):
+    rows = slice(256 * i, 256 * i + 256)
+    og[rows, :] = (nn(tok[rows, :], column(G, 144)) * ssq[rows, :]).astype(BF16)
 
 
 def split_heads(qk, rows):
@@ -328,13 +341,12 @@
 def layer(tokens, gain, wa, wg, cw, conv_gain, wq, wk, wv, wo, wd, bias, extra_t, head_gain, init, woc, wog,
           out, G, tok, Wd, ssq, gext, v, og, qk, dec, extra, Q, within, kv, tots, square, csum, cst, hout, hin, ybuf,
           ztot, zbuf, fbuf, Sst, X, pout, pin, s0, s1, s2, r0, r1, fl, fr, facc,
-          local, hs, hr, cs, cr, ys, yr, zs, zr, fs, fr_, ps, pr, gs, gr, xs, xr_, ds, dr, wzs, wzr, wys, wyr):
+          local, hs, hr, cs, cr, ys, yr, zs, zr, fs, fr_, ps, pr, gs, gr, xs, xr_, ds, dr, wzs, wzr, wys, wyr, wfs, wfr):
     z, y, x, c = (lax.axis_index(n) for n in ("z", "y", "x", "c"))
     sp = z * NY + y
     tp = x * NC + c
-    m = Mover()
-    t = Tokens(m, x, c, tok, ssq, xs, xr_, ds, dr)
-    w = Weights(m, z, y, G, wzs, wzr, wys, wyr)
+    t = Tokens(x, c, tok, ssq, xs, xr_, ds, dr)
+    w = Weights(z, y, G, wzs, wzr, wys, wyr, wfs, wfr)
     own = pltpu.make_async_copy(tokens, tok.at[:, pl.ds(pl.multiple_of(tp * 256, 256), 256)], local)
     own.start()
     pack_chunk(sp, gain, wa, wg, wq, wk, wv, wo, wd, woc, wog, G)
@@ -362,24 +374,30 @@
     t.take(3)
     w.relay(1, PAIRS[2])
     w.forward(1, PAIRS[0])
+    w.begin_z(2)
     for k in (0, 1):
         t.take_across(k)
         t.squares(k, 1 - c)
     w.relay(0, PAIRS[3])
     w.forward(0, PAIRS[2])
-    w.relay(1, PAIRS[3])
+    w.relay(1, PAIRS[3], False)
     w.forward(1, PAIRS[1])
+    w.begin_z(3)
+    w.relay(2, PAIRS[1], False)
     w.relay(0, PAIRS[4])
     w.forward(0, PAIRS[3])
     t.take(4)
     t.take(5)
-    w.relay(1, PAIRS[4])
-    w.begin(2)
+    w.relay(1, PAIRS[4], False)
     for k in (2, 3):
         t.squares(k, c)
         t.take_across(k)
         t.squares(k, 1 - c)
+    w.relay(3, PAIRS[1], False)
+    w.relay(2, PAIRS[2], False)
     w.forward(0, PAIRS[4])
+    w.cross(1, PAIRS[3])
+    w.cross(1, PAIRS[4])
     w.forward(1, PAIRS[2])
     for k in (4, 5):
         t.squares(k, c)
@@ -387,6 +405,8 @@
         t.squares(k, 1 - c)
     t.take(6)
     t.take(7)
+    w.relay(3, PAIRS[2], False)
+    w.relay(2, PAIRS[3], False)
     w.end(0)
     unpack_decay(G, Wd)
     for k in (6, 7):
@@ -396,15 +416,15 @@
 
     for i in range(4):
         project_first(i, tok, G, Wd, ssq, v, qk, dec)
-        if i == 0:
-            w.relay(2, PAIRS[1])
-        if i == 2:
+        if i == 1:
             w.forward(1, PAIRS[3])
+    w.relay(3, PAIRS[3], False)
+    w.relay(2, PAIRS[4], False)
     b2 = jnp.concatenate([bias[...], bias[...]], axis=1)
     for i in range(4):
         block_states(i, b2, extra, dec, qk, v, kv, tots)
         if i == 1:
-            w.relay(2, PAIRS[2])
+            w.forward(1, PAIRS[4])
     tt = tots[...].T[0:64, :]
     decay = jnp.exp(tt)
     state = jnp.zeros((64, 128), F32)
@@ -412,24 +432,17 @@
         state = state * decay[:, b : b + 1] + kv[64 * b : 64 * b + 64, :]
     ybuf[y, 0:64] = state.astype(BF16)
     ybuf[y, 64:128] = jnp.broadcast_to(jnp.exp(jnp.sum(tt, axis=1, keepdims=True)), (64, 128)).astype(BF16)
-    for d in (1, 3, 2):
-        m.send(ybuf.at[y], ys.at[d - 1], yr.at[d - 1], y=lax.rem(y + d, NY))
-    w.forward(1, PAIRS[4])
-    w.relay(2, PAIRS[3])
-    w.end(1)
-
+    for d in (2, 1, 3):
+        send(ybuf.at[y], ys.at[0], yr.at[0], y=lax.rem(y + d, NY))
+    for pair in PAIRS:
+        w.cross(2, pair)
+    for pair in PAIRS[0:4]:
+        w.cross(3, pair)
     for i in range(4):
-        project_second(i, tok, G, ssq, gext, og)
-        if i == 2:
-            w.relay(2, PAIRS[4])
-    hout[...] = gext[ROWS : ROWS + 32, :].astype(BF16)
-    after, ahead = following(z, y, 1), following(z, y, -1)
-    halo = remote(hout, hin, hs.at[0], hr.at[0], **after)
-    halo.start()
-
-    for d in (1, 2, 3):
-        yd = lax.rem(y + NY - d, NY)
-        arrived(ybuf.at[yd], ys.at[0], yr.at[d - 1], y=yd)
+        block_scores(i, dec, qk, v, Q, within)
+    w.relay(3, PAIRS[4])
+
+    arrived(ybuf.at[0:3], yr.at[0], y=lax.rem(y + 1, NY))
     row_state = jnp.zeros((64, 128), F32)
     row_decay = jnp.ones((64, 128), F32)
     pre_state, pre_decay = row_state, row_decay
@@ -445,63 +458,74 @@
     ztot[3] = pre_decay
     part = pl.ds(pl.multiple_of(y * 16, 16), 16)
     zbuf[z, 0:16] = ztot[0, part, :].astype(BF16)
-    zbuf[z, 16:32] = ztot[1, part, :].astype(BF16)
+    low = iota((8, 128), 1) < 64
+    a = ztot[1, part, :]
+    zbuf[z, 16:24] = jnp.where(low, a[0:8], a[8:16]).astype(BF16)
     for d in range(NZ - 1, 0, -1):
         @pl.when(z + d < NZ)
         def _():
             remote(zbuf.at[z], zbuf.at[z], zs.at[d - 1], zr.at[d - 1], z=lax.rem(z + d, NZ)).start()
 
-    block_scores(0, dec, qk, v, Q, within)
-    w.forward(2, PAIRS[0])
-    w.forward(2, PAIRS[1])
+    w.end(1)
+
+    for i in range(4):
+        project_second(i, tok, G, ssq, gext)
+    hout[...] = gext[ROWS : ROWS + 32, :].astype(BF16)
+    after, ahead = following(z, y, 1), following(z, y, -1)
+    halo = remote(hout, hin, hs.at[0], hr.at[0], **after)
+    halo.start()
+
+    for pair in PAIRS:
+        w.forward(2, pair)
     halo.wait_send()
     remote(hout, hin, hs.at[0], hr.at[0], **ahead).wait_recv()
     gext[0:32, :] = jnp.where(sp > 0, hin[...].astype(F32), 0.0)
     conv_sums(cw, gext, csum, cst.at[tp])
     for r in range(1, 8):
-        m.send(cst.at[tp], cs.at[r - 1], cr.at[r - 1], **peer(x, c, r))
-    w.forward(2, PAIRS[2])
-    for i in range(1, 4):
-        block_scores(i, dec, qk, v, Q, within)
-    w.forward(2, PAIRS[3])
-
-    for r in range(1, 8):
-        ids = back_peer(x, c, r)
-        arrived(cst.at[ids["x"] * NC + ids["c"]], cs.at[0], cr.at[r - 1], **ids)
+        send(cst.at[tp], cs.at[0], cr.at[0], **peer(x, c, r))
+    for pair in PAIRS[0:3]:
+        w.forward(3, pair)
+    w.end(2)
+    for i in range(4):
+        project_third(i, tok, G, ssq, og)
+    for pair in PAIRS[3:5]:
+        w.forward(3, pair)
+
+    arrived(cst.at[0:7], cr.at[0], c=1 - c)
     conv_finish(cst, square, csum, conv_gain[...], X)
 
     for d in range(1, NZ):
         @pl.when(z >= d)
         def _():
             zd = lax.rem(z + NZ - d, NZ)
-            arrived(zbuf.at[zd], zs.at[0], zr.at[d - 1], z=zd)
+            arrived(zbuf.at[zd], zr.at[d - 1], z=zd)
     state = init[part, :]
     for k in range(NZ - 1):
-        following_state = state * zbuf[k, 16:32].astype(F32) + zbuf[k, 0:16].astype(F32)
+        a = zbuf[k, 16:24].astype(F32)
+        b = pltpu.roll(a, 64, 1)
+        a = jnp.concatenate([jnp.where(low, a, b), jnp.where(low, b, a)], axis=0)
+        following_state = state * a + zbuf[k, 0:16].astype(F32)
         state = jnp.where(k < z, following_state, state)
     fbuf[y] = state.astype(BF16)
-    for d in (1, 3, 2):
-        m.send(fbuf.at[y], fs.at[d - 1], fr_.at[d - 1], y=lax.rem(y + d, NY))
-    w.forward(2, PAIRS[4])
-    for d in (1, 2, 3):
-        yd = lax.rem(y + NY - d, NY)
-        arrived(fbuf.at[yd], fs.at[0], fr_.at[d - 1], y=yd)
+    for d in (2, 1, 3):
+        send(fbuf.at[y], fs.at[0], fr_.at[0], y=lax.rem(y + d, NY))
+    arrived(fbuf.at[0:3], fr_.at[0], y=lax.rem(y + 1, NY))
     state = fbuf[...].reshape(64, 128).astype(F32) * ztot[3] + ztot[2]
     for b in range(16):
         Sst[64 * b : 64 * b + 64, :] = state.astype(BF16)
         state = state * decay[:, b : b + 1] + kv[64 * b : 64 * b + 64, :]
-    for i in range(4):
-        rows = slice(256 * i, 256 * i + 256)
+
+    def finish(xi):
+        rows = pl.ds(pl.multiple_of(xi * 256, 256), 256)
         attn = within[rows, :] + nn(Q[rows, :], Sst[rows, :])
         mean = jnp.sum(attn * attn, axis=1, keepdims=True) * (1.0 / 128.0)
         o = og[rows, :].astype(F32)
         X[rows, 128:256] = (
             attn * lax.rsqrt(mean + epsilon) * head_gain[...] * (o * jax.nn.sigmoid(o))
         ).astype(BF16)
-    w.end(2)
-
-    right, left, over = lax.rem(x + 1, NX), lax.rem(x + NX - 1, NX), lax.rem(x + 2, NX)
-    order = (over, right, left, x)
+
+    right, back, over = lax.rem(x + 1, NX), lax.rem(x + NX - 1, NX), lax.rem(x + 2, NX)
+    order = (over, right, back, x)
 
     def product(xi, ci, n):
         rows = pl.ds(pl.multiple_of((xi * NC + ci) * 128, 128), 128)
@@ -513,14 +537,12 @@
         return slice(1024 * h, 1024 * h + 1024)
 
     def pair(q, h):
-        return remote(pout.at[q, :, half(h)], pin.at[q, :, half(h)], ps.at[q, h], pr.at[q, h], c=1 - c)
+        return remote(pout.at[q, :, half(h)], pin.at[q, :, half(h)], ps.at[0], pr.at[q, h], c=1 - c)
 
     def for_pair(q, h):
         for n in (2 * h, 2 * h + 1):
             pout[q, :, 512 * n : 512 * n + 512] = product(order[q], 1 - c, n).astype(BF16)
-        copy = pair(q, h)
-        copy.start()
-        m.sent.append(copy)
+        pair(q, h).start()
 
     def pair_sum(q, h, to):
         mine = [product(order[q], c, n) for n in (2 * h, 2 * h + 1)]
@@ -530,52 +552,62 @@
             to[:, cols] = (value + pin[q, :, cols].astype(F32)).astype(to.dtype)
 
     def ring(k, src, dst, xi):
-        copy = remote(src, dst, gs.at[k], gr.at[k], x=xi)
-        copy.start()
-        m.sent.append(copy)
+        remote(src, dst, gs.at[0], gr.at[k], x=xi).start()
 
     def ring_in(k, dst, xi):
-        remote(dst, dst, gs.at[k], gr.at[k], x=xi).wait_recv()
-
+        arrived(dst, gr.at[k], x=xi)
+
+    finish(over)
+    w.end(3)
     for_pair(0, 0)
     for_pair(0, 1)
-    for_pair(1, 1)
+    finish(right)
     pair_sum(0, 0, s0)
     ring(0, s0.at[:, half(0)], r0, right)
+    for_pair(1, 1)
     pair_sum(0, 1, s0)
-    ring(1, s0.at[:, half(1)], r1, left)
+    ring(1, s0.at[:, half(1)], r1, back)
+    finish(back)
     for_pair(2, 0)
     pair_sum(1, 1, s1)
     ring(2, s1.at[:, half(1)], fl.at[:, half(1)], right)
     for_pair(1, 0)
     pair_sum(2, 0, s2)
-    ring(3, s2.at[:, half(0)], fr.at[:, half(0)], left)
+    ring(3, s2.at[:, half(0)], fr.at[:, half(0)], back)
     for_pair(2, 1)
+    finish(x)
     pair_sum(1, 0, s1)
     for_pair(3, 0)
     pair_sum(2, 1, s2)
     for_pair(3, 1)
-    pair_sum(3, 0, facc)
-    pair_sum(3, 1, facc)
-    ring_in(0, r0, left)
+    ring_in(0, r0, back)
     s1[:, half(0)] = (s1[:, half(0)].astype(F32) + r0[...].astype(F32)).astype(BF16)
     ring(4, s1.at[:, half(0)], fl.at[:, half(0)], right)
     ring_in(1, r1, right)
     s2[:, half(1)] = (s2[:, half(1)].astype(F32) + r1[...].astype(F32)).astype(BF16)
-    ring(5, s2.at[:, half(1)], fr.at[:, half(1)], left)
-    ring_in(2, fl.at[:, half(1)], left)
+    ring(5, s2.at[:, half(1)], fr.at[:, half(1)], back)
+    pair_sum(3, 0, facc)
+    pair_sum(3, 1, facc)
+    for p in range(4):
+        w.drain(p)
+    t.drain()
+    left(ybuf.at[0:3], ys.at[0], y=after["y"])
+    left(fbuf.at[0:3], fs.at[0], y=after["y"])
+    left(cst.at[0:7], cs.at[0], c=1 - c)
+    left(pout, ps.at[0], c=1 - c)
+    for d in range(1, NZ):
+        @pl.when(z + d < NZ)
+        def _():
+            left(zbuf.at[z], zs.at[d - 1], z=lax.rem(z + d, NZ))
+    ring_in(2, fl.at[:, half(1)], back)
     ring_in(3, fr.at[:, half(0)], right)
     facc[:, half(0)] += fr[:, half(0)].astype(F32)
     facc[:, half(1)] += fl[:, half(1)].astype(F32)
-    ring_in(4, fl.at[:, half(0)], left)
+    ring_in(4, fl.at[:, half(0)], back)
     out[:, half(0)] = (facc[:, half(0)] + fl[:, half(0)].astype(F32)).astype(BF16)
     ring_in(5, fr.at[:, half(1)], right)
     out[:, half(1)] = (facc[:, half(1)] + fr[:, half(1)].astype(F32)).astype(BF16)
-    m.drain()
-    for d in range(1, NZ):
-        @pl.when(z + d < NZ)
-        def _():
-            remote(zbuf.at[z], zbuf.at[z], zs.at[d - 1], zr.at[d - 1], z=lax.rem(z + d, NZ)).wait_send()
+    left(pout.at[0:3], gs.at[0], x=right)
 
 
 def per_device(
@@ -589,12 +621,15 @@
         ((ROWS, 128), BF16), ((ROWS, 128), BF16), ((ROWS, 128), F32), ((ROWS, 128), F32), ((ROWS, 128), F32),
         ((ROWS, 256), BF16), ((ROWS, 128), F32), ((ROWS, 128), F32), ((128, 128), F32), ((128, 128), F32),
         ((ROWS, 128), F32), ((8, 16, 128), F32), ((32, 128), BF16), ((32, 128), BF16), ((NY, 128, 128), BF16),
-        ((4, 64, 128), F32), ((NZ, 32, 128), BF16), ((NY, 16, 128), BF16), ((ROWS, 128), BF16), ((ROWS, 256), BF16),
+        ((4, 64, 128), F32), ((NZ, 24, 128), BF16), ((NY, 16, 128), BF16), ((ROWS, 128), BF16), ((ROWS, 256), BF16),
         ((4, 128, D), BF16), ((4, 128, D), BF16), ((128, D), BF16), ((128, D), BF16), ((128, D), BF16),
         ((128, 1024), BF16), ((128, 1024), BF16), ((128, D), BF16), ((128, D), BF16), ((128, D), F32),
     ]
-    counts = [(1,), (7,), (3,), (15,), (3,), (4, 2), (6,), (6,), (8,), (3, 16), (3, 16, 4)]
-    scratch = [pltpu.VMEM(s, t) for s, t in shapes] + [dma] + [dma(n) for n in counts for _ in (0, 1)]
+    counts = [
+        (1,), (1,), (1,), (1,), (1,), (1,), (15,), (15,), (1,), (1,), (1,), (4, 2), (1,), (6,),
+        (1,), (6,), (1,), (8,), (4,), (4, 16), (4,), (4, 9, 2), (4,), (4,),
+    ]
+    scratch = [pltpu.VMEM(s, t) for s, t in shapes] + [dma] + [dma(n) for n in counts]
     return pl.pallas_call(
         layer,
         out_shape=jax.ShapeDtypeStruct((128, D), BF16),

time: 98.6 us -> 90.2 us (0.915)
  Pallas kernels: 96.5 us -> 88.1 us
    pallas_call x1, Pallas kernels: 96.5 us -> 88.1 us  [per_device(): pl.pallas_call(layer, out_shape=jax.ShapeDtypeStruct((128, D), BF16), in_...]
where the time goes in v4:
time: 90.2 us; the launch traced here: 90 us
  Pallas kernels  88.1 us (98%)
  local copies, waits for them, and re-layouts  1.88 us (2%)
    pallas_call x1, Pallas kernels, per_device(): pl.pallas_call(layer, out_shape=jax.ShapeDtypeStruct((128, D), BF16), in_...  88.1 us
    unnamed x1, local copies, waits for them, and re-layouts  1.88 us

profile of v4, /device:TPU:1, one launch (start us, length us, event | category | flops | bytes accessed | tf_op | source)
XLA Modules:
  0.0 90.0 jit_solution(6236191707812323885)
XLA Ops:
  0.0 88.1 %shard_map.163 = bf16[128,2048]{1,0:T(8,128)(2,1)} custom-call(bf16[1024,256]{1,0:T(8,128)(2,1)} %tokens.1, f32[16,128]{1,0:T(8,128)} %bitcast.10, bf16[32,128]{1,0:T(8,128)(2,1)} %wa.1, bf16[32,128]{1,0:T(8,128)(2,1)} %wg.1, f32[31,128]{1,0:T(8,128)} %cw.1, f32[1,128]{1,0:T(1,128)} %bitcast.13, bf16[32,64]{1,0:T(8,128)(2,1)} %wq.1, bf16[32,64]{1,0:T(8,128)(2,1)} %wk.1, ...), custom_call_target="tpu_custom_call" | custom-call | tf_op jit(solution)/shard_map/pallas_call | solution.py:633
  88.1 1.9 %copy.19 = bf16[128,2048]{1,0:T(8,128)(2,1)} copy(bf16[128,2048]{1,0:T(8,128)(2,1)} %shard_map.163) | data formatting | bytes 1048576

commit v5 on v4

--- a/solution.py
+++ b/solution.py
@@ -14,8 +14,9 @@
 SP = ("z", "y")
 TP = ("x", "c")
 SP_TP = ("z", "y", "x", "c")
-PARTS = ((0, 80), (80, 144), (144, 176), (176, 240))
+PARTS = ((0, 80), (80, 144), (144, 176), (208, 240), (176, 208))
 PAIRS = ((0,), (1, 2), (3, 4), (5, 6), (7, 8))
+EARLY, LATE = (0, 1, 2, 5, 6, 7, 8, 9, 14, 15), (3, 4, 10, 11, 12, 13)
 F32, BF16 = jnp.float32, jnp.bfloat16
 
 epsilon = 1e-06
@@ -66,7 +67,8 @@
     G[sp, 208:240] = wog[...]
 
 
-def greet(z, y, x, c):
+def greet_all():
+    z, y, x, c = (lax.axis_index(n) for n in ("z", "y", "x", "c"))
     barrier = pltpu.get_barrier_semaphore()
     partners = [dict(z=lax.rem(z + d, NZ)) for d in (1, 2, NZ - 2, NZ - 1)]
     partners += [dict(y=lax.rem(y + d, NY)) for d in (1, NY - 1)]
@@ -74,7 +76,10 @@
     partners += [dict(c=1 - c)]
     for ids in partners:
         pl.semaphore_signal(barrier, inc=1, device_id=ids, device_id_type=pl.DeviceIdType.MESH)
-    pl.semaphore_wait(barrier, len(partners))
+
+
+def greet_wait():
+    pl.semaphore_wait(pltpu.get_barrier_semaphore(), 9)
 
 
 def peer(x, c, r):
@@ -150,6 +155,34 @@
 
     def end(self, p):
         arrived(self.several(p, 16), self.fr.at[p], y=self.down)
+
+    def row(self, o):
+        return self.G.at[pl.ds(lax.rem(self.z - o + NZ, NZ) * NY, NY), PARTS[4][0] : PARTS[4][1]]
+
+    def row_out(self, o):
+        step = (2 if abs(o) > 1 else 1) * (1 if o > 0 else -1)
+        send(self.row(o - step), self.zs.at[4], self.zr.at[4, o + 7], z=lax.rem(self.z + step + NZ, NZ))
+
+    def rows_y(self):
+        for to in (self.over, self.up, self.down):
+            send(self.chunk(0, self.y, *PARTS[4]), self.ys.at[4], self.yr.at[4, 0, 0], y=to)
+
+    def rows_begin(self):
+        arrived(self.several(4, 3), self.yr.at[4, 0, 0], y=self.up)
+        for o in (1, -1, 2, -2):
+            self.row_out(o)
+
+    def rows_relay(self, pair):
+        for a in pair:
+            for o in self.signs(a):
+                arrived(self.row(o), self.zr.at[4, o + 7], z=lax.rem(self.z + 1, NZ))
+                further = o + 2 if o > 0 else o - 2
+                if -7 <= further <= 8:
+                    self.row_out(further)
+
+    def rows_drain(self):
+        left(self.several(4, 60), self.zs.at[4], y=self.down)
+        left(self.several(4, 3), self.ys.at[4], y=self.down)
 
     def drain(self, p):
         left(self.several(p, 15), self.zs.at[p], y=self.down)
@@ -313,15 +346,14 @@
     within[rows, :] = nn(scores, v[rows, :])
 
 
-def conv_sums(cw, gext, csum, mine):
-    for b in range(8):
-        acc = jnp.zeros((128, 128), F32)
-        for j in range(TAPS):
-            acc = acc + cw[j : j + 1, :] * gext[128 * b + 2 + j : 128 * b + 130 + j, :]
-        csum[128 * b : 128 * b + 128, :] = acc
-        t = acc.T
-        mine[b : b + 1, :] = jnp.sum(t, axis=0, keepdims=True)
-        mine[8 + b : 9 + b, :] = jnp.sum(t * t, axis=0, keepdims=True)
+def conv_sums(b, cw, gext, csum, mine):
+    acc = jnp.zeros((128, 128), F32)
+    for j in range(TAPS):
+        acc = acc + cw[j : j + 1, :] * gext[128 * b + 2 + j : 128 * b + 130 + j, :]
+    csum[128 * b : 128 * b + 128, :] = acc
+    t = acc.T
+    mine[b : b + 1, :] = jnp.sum(t, axis=0, keepdims=True)
+    mine[8 + b : 9 + b, :] = jnp.sum(t * t, axis=0, keepdims=True)
 
 
 def conv_finish(cst, square, csum, conv_gain, X):
@@ -338,7 +370,17 @@
         X[128 * b : 128 * b + 128, 0:128] = (n * jax.nn.sigmoid(n)).astype(BF16)
 
 
-def layer(tokens, gain, wa, wg, cw, conv_gain, wq, wk, wv, wo, wd, bias, extra_t, head_gain, init, woc, wog,
+def layer(*refs):
+    tokens, given, out = refs[0], refs[1:17], refs[17]
+    held, in_sems, rest = refs[18:34], refs[34], refs[35:]
+    greet_all()
+    copies = [pltpu.make_async_copy(a, b, in_sems.at[k]) for k, (a, b) in enumerate(zip(given, held))]
+    for k in EARLY + LATE:
+        copies[k].start()
+    run_layer(copies, tokens, *held, out, *rest)
+
+
+def run_layer(copies, tokens, gain, wa, wg, cw, conv_gain, wq, wk, wv, wo, wd, bias, extra_t, head_gain, init, woc, wog,
           out, G, tok, Wd, ssq, gext, v, og, qk, dec, extra, Q, within, kv, tots, square, csum, cst, hout, hin, ybuf,
           ztot, zbuf, fbuf, Sst, X, pout, pin, s0, s1, s2, r0, r1, fl, fr, facc,
           local, hs, hr, cs, cr, ys, yr, zs, zr, fs, fr_, ps, pr, gs, gr, xs, xr_, ds, dr, wzs, wzr, wys, wyr, wfs, wfr):
@@ -349,14 +391,18 @@
     w = Weights(z, y, G, wzs, wzr, wys, wyr, wfs, wfr)
     own = pltpu.make_async_copy(tokens, tok.at[:, pl.ds(pl.multiple_of(tp * 256, 256), 256)], local)
     own.start()
+    for k in EARLY:
+        copies[k].wait()
     pack_chunk(sp, gain, wa, wg, wq, wk, wv, wo, wd, woc, wog, G)
     zbuf[...] = jnp.zeros_like(zbuf)
-    greet(z, y, x, c)
+    greet_wait()
 
     w.begin(0)
     own.wait()
     t.begin()
     w.begin(1)
+    for k in LATE:
+        copies[k].wait()
     for b in range(8):
         e = extra_t[:, 128 * b : 128 * b + 128]
         extra[128 * b : 128 * b + 128, :] = jnp.concatenate([e, e], axis=0).T
@@ -375,6 +421,7 @@
     w.relay(1, PAIRS[2])
     w.forward(1, PAIRS[0])
     w.begin_z(2)
+    w.rows_y()
     for k in (0, 1):
         t.take_across(k)
         t.squares(k, 1 - c)
@@ -395,6 +442,7 @@
         t.squares(k, 1 - c)
     w.relay(3, PAIRS[1], False)
     w.relay(2, PAIRS[2], False)
+    w.rows_begin()
     w.forward(0, PAIRS[4])
     w.cross(1, PAIRS[3])
     w.cross(1, PAIRS[4])
@@ -413,18 +461,19 @@
         t.squares(k, c)
         t.take_across(k)
         t.squares(k, 1 - c)
+    w.forward(1, PAIRS[3])
 
     for i in range(4):
         project_first(i, tok, G, Wd, ssq, v, qk, dec)
         if i == 1:
-            w.forward(1, PAIRS[3])
+            w.forward(1, PAIRS[4])
+            w.rows_relay(PAIRS[1])
     w.relay(3, PAIRS[3], False)
     w.relay(2, PAIRS[4], False)
     b2 = jnp.concatenate([bias[...], bias[...]], axis=1)
     for i in range(4):
         block_states(i, b2, extra, dec, qk, v, kv, tots)
-        if i == 1:
-            w.forward(1, PAIRS[4])
+    w.rows_relay(PAIRS[2])
     tt = tots[...].T[0:64, :]
     decay = jnp.exp(tt)
     state = jnp.zeros((64, 128), F32)
@@ -438,9 +487,15 @@
         w.cross(2, pair)
     for pair in PAIRS[0:4]:
         w.cross(3, pair)
-    for i in range(4):
-        block_scores(i, dec, qk, v, Q, within)
-    w.relay(3, PAIRS[4])
+    w.end(1)
+
+    after, ahead = following(z, y, 1), following(z, y, -1)
+    halo = remote(hout, hin, hs.at[0], hr.at[0], **after)
+    for i in (3, 0, 1, 2):
+        project_second(i, tok, G, ssq, gext)
+        if i == 3:
+            hout[...] = gext[ROWS : ROWS + 32, :].astype(BF16)
+            halo.start()
 
     arrived(ybuf.at[0:3], yr.at[0], y=lax.rem(y + 1, NY))
     row_state = jnp.zeros((64, 128), F32)
@@ -466,33 +521,23 @@
         def _():
             remote(zbuf.at[z], zbuf.at[z], zs.at[d - 1], zr.at[d - 1], z=lax.rem(z + d, NZ)).start()
 
-    w.end(1)
-
-    for i in range(4):
-        project_second(i, tok, G, ssq, gext)
-    hout[...] = gext[ROWS : ROWS + 32, :].astype(BF16)
-    after, ahead = following(z, y, 1), following(z, y, -1)
-    halo = remote(hout, hin, hs.at[0], hr.at[0], **after)
-    halo.start()
-
-    for pair in PAIRS:
+    w.relay(3, PAIRS[4])
+    w.rows_relay(PAIRS[3])
+    for pair in PAIRS[0:3]:
         w.forward(2, pair)
-    halo.wait_send()
-    remote(hout, hin, hs.at[0], hr.at[0], **ahead).wait_recv()
+    for b in range(1, 8):
+        conv_sums(b, cw, gext, csum, cst.at[tp])
+    arrived(hin, hr.at[0], **ahead)
     gext[0:32, :] = jnp.where(sp > 0, hin[...].astype(F32), 0.0)
-    conv_sums(cw, gext, csum, cst.at[tp])
+    conv_sums(0, cw, gext, csum, cst.at[tp])
     for r in range(1, 8):
         send(cst.at[tp], cs.at[0], cr.at[0], **peer(x, c, r))
+    for pair in PAIRS[3:5]:
+        w.forward(2, pair)
     for pair in PAIRS[0:3]:
         w.forward(3, pair)
-    w.end(2)
     for i in range(4):
-        project_third(i, tok, G, ssq, og)
-    for pair in PAIRS[3:5]:
-        w.forward(3, pair)
-
-    arrived(cst.at[0:7], cr.at[0], c=1 - c)
-    conv_finish(cst, square, csum, conv_gain[...], X)
+        block_scores(i, dec, qk, v, Q, within)
 
     for d in range(1, NZ):
         @pl.when(z >= d)
@@ -509,6 +554,16 @@
     fbuf[y] = state.astype(BF16)
     for d in (2, 1, 3):
         send(fbuf.at[y], fs.at[0], fr_.at[0], y=lax.rem(y + d, NY))
+    w.end(2)
+    for i in range(4):
+        project_third(i, tok, G, ssq, og)
+    for pair in PAIRS[3:5]:
+        w.forward(3, pair)
+    w.rows_relay(PAIRS[4])
+
+    arrived(cst.at[0:7], cr.at[0], c=1 - c)
+    conv_finish(cst, square, csum, conv_gain[...], X)
+
     arrived(fbuf.at[0:3], fr_.at[0], y=lax.rem(y + 1, NY))
     state = fbuf[...].reshape(64, 128).astype(F32) * ztot[3] + ztot[2]
     for b in range(16):
@@ -590,6 +645,8 @@
     pair_sum(3, 1, facc)
     for p in range(4):
         w.drain(p)
+    w.rows_drain()
+    halo.wait_send()
     t.drain()
     left(ybuf.at[0:3], ys.at[0], y=after["y"])
     left(fbuf.at[0:3], fs.at[0], y=after["y"])
@@ -627,23 +684,24 @@
     ]
     counts = [
         (1,), (1,), (1,), (1,), (1,), (1,), (15,), (15,), (1,), (1,), (1,), (4, 2), (1,), (6,),
-        (1,), (6,), (1,), (8,), (4,), (4, 16), (4,), (4, 9, 2), (4,), (4,),
+        (1,), (6,), (1,), (8,), (5,), (5, 16), (5,), (5, 9, 2), (5,), (5,),
     ]
     scratch = [pltpu.VMEM(s, t) for s, t in shapes] + [dma] + [dma(n) for n in counts]
+    args = (
+        norm_gain.reshape(16, 128), w_conv_a, w_conv_gate, conv_weight, conv_gain.reshape(1, 128),
+        w_query, w_key, w_value, w_outgate, w_decay, decay_bias.reshape(1, 64), decay_extra.T,
+        head_gain.reshape(1, 128), init_state.reshape(64, 128), w_out_conv.T, w_out_gla.T,
+    )
     return pl.pallas_call(
         layer,
         out_shape=jax.ShapeDtypeStruct((128, D), BF16),
-        in_specs=[pl.BlockSpec(memory_space=pl.ANY)] + [vm] * 16,
+        in_specs=[pl.BlockSpec(memory_space=pl.ANY)] * 17,
         out_specs=vm,
-        scratch_shapes=scratch,
+        scratch_shapes=[pltpu.VMEM(a.shape, a.dtype) for a in args] + [dma((16,))] + scratch,
         compiler_params=pltpu.CompilerParams(
             collective_id=0, has_side_effects=True, vmem_limit_bytes=60 * 1024 * 1024
         ),
-    )(
-        tokens, norm_gain.reshape(16, 128), w_conv_a, w_conv_gate, conv_weight, conv_gain.reshape(1, 128),
-        w_query, w_key, w_value, w_outgate, w_decay, decay_bias.reshape(1, 64), decay_extra.T,
-        head_gain.reshape(1, 128), init_state.reshape(64, 128), w_out_conv.T, w_out_gla.T,
-    )
+    )(tokens, *args)
 
 
 def solution(mesh):

time: 90.2 us -> 87.4 us (0.969)
  Pallas kernels: 88.1 us -> 85.3 us
    pallas_call x1, Pallas kernels: 88.1 us -> 85.3 us  [per_device(): pl.pallas_call(layer, out_shape=jax.ShapeDtypeStruct((128, D), BF16), in_...]
where the time goes in v5:
time: 87.4 us; the launch traced here: 87.2 us
  Pallas kernels  85.3 us (98%)
  local copies, waits for them, and re-layouts  1.88 us (2%)
    pallas_call x1, Pallas kernels, per_device(): pl.pallas_call(layer, out_shape=jax.ShapeDtypeStruct((128, D), BF16), in_...  85.3 us
    unnamed x1, local copies, waits for them, and re-layouts  1.88 us

profile of v5, /device:TPU:1, one launch (start us, length us, event | category | flops | bytes accessed | tf_op | source)
XLA Modules:
  0.0 87.2 jit_solution(11112286859514469673)
XLA Ops:
  0.0 85.3 %shard_map.163 = bf16[128,2048]{1,0:T(8,128)(2,1)} custom-call(bf16[1024,256]{1,0:T(8,128)(2,1)} %refs_0_.1, f32[16,128]{1,0:T(8,128)} %bitcast.10, bf16[32,128]{1,0:T(8,128)(2,1)} %refs_2_.1, bf16[32,128]{1,0:T(8,128)(2,1)} %refs_3_.1, f32[31,128]{1,0:T(8,128)} %refs_4_.1, f32[1,128]{1,0:T(1,128)} %bitcast.13, bf16[32,64]{1,0:T(8,128)(2,1)} %refs_6_.1, ...), custom_call_target="tpu_custom_call" | custom-call | tf_op jit(solution)/shard_map/pallas_call | solution.py:695
  85.3 1.9 %copy.19 = bf16[128,2048]{1,0:T(8,128)(2,1)} copy(bf16[128,2048]{1,0:T(8,128)(2,1)} %shard_map.163) | data formatting | bytes 1048576
